TPU v7x, 32 devices: a whole 2x2x4 slice. The times are simulated.
32 devices in a mesh: ep: 8 (over z, core), tp: 4 (over y, x).
Axes of the slice: x: 2, y: 2, z: 4, core: 2. Of those that a mesh axis runs over, the one named last changes fastest.
Arguments:
- tokens: bfloat16 [1024, 2048], P('ep'), may hold values from -6 to 6
- cotangent: bfloat16 [1024, 2048], P('ep'), may hold values from -6 to 6
- expert_ids: int32 [1024, 2], P('ep'), may hold values from 0 to 7, all different within a row; in each aligned block of 128 rows (0 to 127, 128 to 255, ...) at most 64 rows name the same one
- route_weight: bfloat16 [1024, 2], P('ep'), may hold values from 0.19921875 to 1
- gate_weight: bfloat16 [8, 1024, 2048], P('ep', 'tp'), may hold values from -0.125 to 0.125
- up_weight: bfloat16 [8, 1024, 2048], P('ep', 'tp'), may hold values from -0.125 to 0.125
- down_weight: bfloat16 [8, 1024, 2048], P('ep', 'tp'), may hold values from -0.1875 to 0.1875
Outputs:
- tokens_grad: bfloat16 [1024, 2048], P('ep', 'tp')
- route_weight_grad: float32 [1024, 2], P('ep')
- gate_weight_grad: float32 [8, 1024, 2048], P('ep', 'tp')
- up_weight_grad: float32 [8, 1024, 2048], P('ep', 'tp')
- down_weight_grad: float32 [8, 1024, 2048], P('ep', 'tp')
Inputs may be any that keep to these rules, and one draw needn't show every extreme that they name: `expert_ids`: within each aligned block of 128 rows every expert is named at most 64 times; the two experts of a row differ.
All inputs are finite; a program needn't handle non-finite values.
Results may differ from a plain program's by a relative error of at most 0.0058.
Values may be sent and summed in bfloat16 or wider, within the bound.
A program may use at most 64 MiB of HBM per device.

v0:
```python
import functools

import jax
import jax.numpy as jnp
from jax import lax
from jax.experimental import pallas as pl
from jax.experimental.pallas import tpu as pltpu
from jax.sharding import PartitionSpec as P

MESH = pl.DeviceIdType.MESH
F32 = jnp.float32
BF16 = jnp.bfloat16


def slices_for(j, tp, bits, count):
    base = j
    for bit in bits:
        base = base - ((j // bit) % 2) * bit
    out = []
    for k in range(count):
        out.append(base + sum(bit for n, bit in enumerate(bits) if (k >> n) & 1))
    return out


def kernel(
    ep, tp, tokens, cotangent, ids, probs, gate_w, up_w, down_w,
    dx_out, route_out, gate_out, up_out, down_out,
    rows, weights, pair_w, wg, part, core_in, tp_in, z_in, grads, totals, r_send, r_in, r_tp,
    load_sem, wz_send, wz_recv, z_send, z_recv, t_send, t_recv, c_send, c_recv,
    pc_send, pc_recv, pt_send, pt_recv, pz_send, pz_recv, rs_send, rs_recv, rt_send, rt_recv, out_sem,
):
    e, j = lax.axis_index("ep"), lax.axis_index("tp")
    levels = ep // 2
    lvl, core = e // 2, e % 2
    t_rows, width = tokens.shape
    span = width // tp
    half = t_rows // 2
    f_rows = gate_w.shape[0]
    nb = tp.bit_length() - 1
    slots = part.shape[0]
    mate = 2 * lvl + 1 - core

    def order(i):
        near = jnp.minimum(lvl, levels - 1 - lvl)
        d = (i + 1) // 2
        close = jnp.where(i % 2 == 1, lvl - d, lvl + d)
        far = jnp.where(lvl == near, lvl + (i - near), lvl - (i - near))
        return jnp.where(i <= 2 * near, close, far)

    def row0(l, c):
        return pl.multiple_of((2 * l + c) * t_rows, t_rows)

    def col(s):
        return pl.ds(pl.multiple_of(s * span, span), span)

    def flip(bit):
        return j + bit * (1 - 2 * ((j // bit) % 2))

    def remote(src, dst, ssem, rsem, de, dt):
        return pltpu.make_async_remote_copy(
            src_ref=src, dst_ref=dst, send_sem=ssem, recv_sem=rsem,
            device_id=(de, dt), device_id_type=MESH)

    own = pl.ds(row0(lvl, core), t_rows)
    loads = [
        pltpu.make_async_copy(tokens, rows.at[0, own], load_sem.at[0]),
        pltpu.make_async_copy(cotangent, rows.at[1, own], load_sem.at[1]),
        pltpu.make_async_copy(gate_w, weights.at[0], load_sem.at[2]),
        pltpu.make_async_copy(up_w, weights.at[1], load_sem.at[3]),
        pltpu.make_async_copy(down_w, weights.at[2], load_sem.at[4]),
    ]
    for copy in loads:
        copy.start()
    barrier = pltpu.get_barrier_semaphore()

    def greet(n, _):
        pl.semaphore_signal(barrier, inc=1, device_id=(lax.rem(e + n, ep), j), device_id_type=MESH)
        return 0

    def greet_tp(n, _):
        pl.semaphore_signal(barrier, inc=1, device_id=(e, lax.rem(j + n, tp)), device_id_type=MESH)
        return 0

    lax.fori_loop(1, ep, greet, 0)
    lax.fori_loop(1, tp, greet_tp, 0)
    pl.semaphore_wait(barrier, ep + tp - 2)

    def w_copy(d):
        return remote(pair_w.at[d], wg.at[e], wz_send.at[d], wz_recv.at[e], d, j)

    def w_wait(src):
        return remote(pair_w.at[src], wg.at[src], wz_send.at[src], wz_recv.at[src], src, j)

    def z_copy(a, l, side):
        ref = rows.at[a, pl.ds(row0(l, core), t_rows), col(j)]
        de = lax.rem(e + (2 if side else ep - 2), ep)
        return remote(ref, ref, z_send.at[a, side, l], z_recv.at[a, l], de, j)

    def gather_step(a, l, s, receive):
        copies = []
        for h in range(2):
            order_bits = [1 << b for b in (range(nb) if h == 0 else range(nb - 1, -1, -1))]
            peer = flip(order_bits[s])
            ids = slices_for(peer if receive else j, tp, order_bits[:s], 1 << s)
            for k, sid in enumerate(ids):
                ref = rows.at[a, pl.ds(row0(l, core) + h * half, half), col(sid)]
                copies.append(remote(
                    ref, ref, t_send.at[a, l, h, (1 << s) - 1 + k], t_recv.at[a, l, h, sid], e, peer))
        return copies

    def core_copy(a, l, c):
        ref = rows.at[a, pl.ds(row0(l, c), t_rows)]
        return remote(ref, ref, c_send.at[a, l], c_recv.at[a, l], mate, j)

    def pc_copy(l, i):
        return remote(part.at[i % slots, 1 - core], core_in.at[l], pc_send.at[l], pc_recv.at[l], mate, j)

    def scatter_step(l, i, s, receive):
        copies = []
        base = sum(tp >> (n + 1) for n in range(s))
        count = tp >> (s + 1)
        for h in range(2):
            order_bits = [1 << b for b in (range(nb) if h == 0 else range(nb - 1, -1, -1))]
            peer = flip(order_bits[s])
            ids = slices_for(j if receive else peer, tp, order_bits[s + 1:], count)
            for k, sid in enumerate(ids):
                src = part.at[i % slots, core, pl.ds(h * half, half), col(sid)]
                dst = tp_in.at[l, h, base + k]
                copies.append((remote(src, dst, pt_send.at[l, h, base + k], pt_recv.at[l, h, base + k], e, peer),
                               src, dst))
        return copies

    def pz_copy(l, i):
        return remote(part.at[i % slots, core, :, col(j)], z_in.at[lvl], pz_send.at[l], pz_recv.at[lvl],
                      2 * l + core, j)

    def pz_wait(src):
        return remote(part.at[0, core, :, col(j)], z_in.at[src], pz_send.at[src], pz_recv.at[src],
                      2 * src + core, j)

    def pair_row(d, _):
        pair_w[d] = jnp.sum(
            jnp.where(ids[...] == d, probs[...].astype(F32), 0.0), axis=0, keepdims=True)
        return 0

    for n in range(2):
        loads[n].wait()
        @pl.when(lvl + 1 < levels)
        def _():
            z_copy(n, lvl, 1).start()
        @pl.when(lvl > 0)
        def _():
            z_copy(n, lvl, 0).start()
        core_copy(n, lvl, core).start()

    lax.fori_loop(0, ep, pair_row, 0)

    def w_start(n, _):
        w_copy(lax.rem(e + n, ep)).start()
        return 0

    lax.fori_loop(1, ep, w_start, 0)
    wg[e] = pair_w[e]
    for n in range(2, 5):
        loads[n].wait()

    def arrive(i):
        l = order(i)
        for a in range(2):
            z_copy(a, l, 0).wait_recv()
            @pl.when(jnp.logical_and(l < lvl, lvl + 1 < levels))
            def _():
                z_copy(a, l, 1).start()
            @pl.when(jnp.logical_and(l > lvl, lvl > 0))
            def _():
                z_copy(a, l, 0).start()
            for copy in gather_step(a, l, 0, False):
                copy.start()

    def spread(i, s):
        l = order(i)
        for a in range(2):
            for copy in gather_step(a, l, s - 1, True):
                copy.wait_recv()
            if s < nb:
                for copy in gather_step(a, l, s, False):
                    copy.start()
            else:
                core_copy(a, l, core).start()

    def compute(i):
        l = order(i)
        for a in range(2):
            core_copy(a, l, 1 - core).wait_recv()
        @pl.when(l != lvl)
        def _():
            w_wait(2 * l).wait_recv()
            w_wait(2 * l + 1).wait_recv()
        @pl.when(l == lvl)
        def _():
            w_wait(mate).wait_recv()
        sel = pl.ds(row0(l, 0), 2 * t_rows)
        nt = (((1,), (1,)), ((), ()))
        x = rows[0, sel, :]
        pre_gate = lax.dot_general(weights[0], x, nt, preferred_element_type=F32)
        pre_up = lax.dot_general(weights[1], x, nt, preferred_element_type=F32)
        back = lax.dot_general(weights[2], rows[1, sel, :], nt, preferred_element_type=F32)
        p = jnp.concatenate([wg[2 * l], wg[2 * l + 1]], axis=1)
        sigma = jax.nn.sigmoid(pre_gate)
        silu = pre_gate * sigma
        hidden = silu * pre_up
        prod = jnp.sum(hidden * back, axis=0, keepdims=True)
        r_send[2 * l] = prod[:, :t_rows]
        r_send[2 * l + 1] = prod[:, t_rows:]
        scaled = p * back
        gg = (scaled * pre_up * sigma * (1.0 + pre_gate * (1.0 - sigma))).astype(BF16)
        gu = (scaled * silu).astype(BF16)
        grads[0, :, sel] = gg
        grads[1, :, sel] = gu
        grads[2, :, sel] = (p * hidden).astype(BF16)
        ggt, gut = gg.T, gu.T
        tile = min(width, 512)

        def column(n, _):
            cs = pl.ds(pl.multiple_of(n * tile, tile), tile)
            d = (jnp.dot(ggt, weights[0, :, cs], preferred_element_type=F32)
                 + jnp.dot(gut, weights[1, :, cs], preferred_element_type=F32)).astype(BF16)
            part[i % slots, 0, :, cs] = d[:t_rows]
            part[i % slots, 1, :, cs] = d[t_rows:]
            return 0

        lax.fori_loop(0, width // tile, column, 0)
        pc_copy(l, i).start()

        def send_r(d):
            remote(r_send.at[d], r_in.at[e], rs_send.at[d], rs_recv.at[e], d, j).start()
        for c in range(2):
            @pl.when(2 * l + c != e)
            def _():
                send_r(2 * l + c)
            @pl.when(2 * l + c == e)
            def _():
                r_in[2 * l + c] = r_send[2 * l + c]

    def merge_core(i):
        l = order(i)
        pc_copy(l, i).wait()
        part[i % slots, core] = (part[i % slots, core].astype(F32) + core_in[l].astype(F32)).astype(BF16)
        for copy, _, _ in scatter_step(l, i, 0, False):
            copy.start()

    def merge_tp(i, s):
        l = order(i)
        for (copy, _, _), (_, mine, got) in zip(scatter_step(l, i, s, False), scatter_step(l, i, s, True)):
            copy.wait()
            mine[...] = (mine[...].astype(F32) + got[...].astype(F32)).astype(BF16)
        if s + 1 < nb:
            for copy, _, _ in scatter_step(l, i, s + 1, False):
                copy.start()
        else:
            @pl.when(l != lvl)
            def _():
                pz_copy(l, i).start()
            @pl.when(l == lvl)
            def _():
                z_in[lvl] = part[i % slots, core, :, col(j)]

    def drain(i):
        l = order(i)
        @pl.when(l != lvl)
        def _():
            pz_copy(l, i).wait_send()

    outs = (gate_out, up_out, down_out)

    def out_copy(k):
        return pltpu.make_async_copy(totals.at[k], outs[k], out_sem.at[k])

    def weight_grad(k):
        tile = min(width, 512)

        def column(n, _):
            cs = pl.ds(pl.multiple_of(n * tile, tile), tile)
            totals[k, :, cs] = jnp.dot(
                grads[k], rows[k // 2, :, cs], preferred_element_type=F32).astype(BF16)
            return 0

        lax.fori_loop(0, width // tile, column, 0)
        out_copy(k).start()

    compute(0)
    d_comp = nb + 1
    last = levels - 1 + d_comp

    def tick(t, _):
        def stage(f, i, low):
            @pl.when(jnp.logical_and(i >= low, i < levels))
            def _():
                f(i)
        def back(late):
            return jnp.where(t == 1 + late, 0, jnp.where(t > d_comp + late, t - d_comp - late, -1))

        for k in range(3):
            @pl.when(t == last + k)
            def _():
                weight_grad(k)
        stage(drain, back(nb + 1), 0)
        for s in range(nb, 0, -1):
            stage(functools.partial(spread, s=s), t - s, 1)
        stage(arrive, t, 1)
        for s in range(nb - 1, -1, -1):
            stage(functools.partial(merge_tp, s=s), back(1 + s), 0)
        stage(compute, t - d_comp + 1, 1)
        stage(merge_core, back(0), 0)
        return 0

    lax.fori_loop(1, levels + d_comp + nb + 1, tick, 0)

    def r_wait(n, _):
        src = lax.rem(e + n, ep)
        remote(r_send.at[src], r_in.at[src], rs_send.at[src], rs_recv.at[src], src, j).wait()
        return 0

    lax.fori_loop(1, ep, r_wait, 0)

    def rt_copy(n):
        dt = lax.rem(j + n, tp)
        return remote(r_in, r_tp.at[j], rt_send.at[dt], rt_recv.at[j], e, dt)

    def rt_wait(n, _):
        src = lax.rem(j + n, tp)
        remote(r_in, r_tp.at[src], rt_send.at[src], rt_recv.at[src], e, src).wait()
        return 0

    def rt_start(n, _):
        rt_copy(n).start()
        return 0

    lax.fori_loop(1, tp, rt_start, 0)
    r_tp[j] = r_in[...]

    def pz_drain(src, _):
        @pl.when(src != lvl)
        def _():
            pz_wait(src).wait_recv()
        return 0

    lax.fori_loop(0, levels, pz_drain, 0)
    dx_out[...] = jnp.sum(z_in[...].astype(F32), axis=0).astype(BF16)
    lax.fori_loop(1, tp, rt_wait, 0)
    r_in[...] = jnp.sum(r_tp[...], axis=0)

    def choose(d, acc):
        return acc + jnp.where(ids[...] == d, r_in[d], 0.0)

    route_out[...] = lax.fori_loop(0, ep, choose, jnp.zeros(route_out.shape, F32))

    for a in range(2):
        @pl.when(lvl + 1 < levels)
        def _():
            z_copy(a, lvl, 1).wait_send()
        @pl.when(lvl > 0)
        def _():
            z_copy(a, lvl, 0).wait_send()

    def finish(l, _):
        for a in range(2):
            core_copy(a, l, core).wait_send()
            @pl.when(jnp.logical_and(l < lvl, lvl + 1 < levels))
            def _():
                z_copy(a, l, 1).wait_send()
            @pl.when(jnp.logical_and(l > lvl, lvl > 0))
            def _():
                z_copy(a, l, 0).wait_send()
            @pl.when(l != lvl)
            def _():
                for s in range(nb):
                    for copy in gather_step(a, l, s, False):
                        copy.wait_send()
        return 0

    lax.fori_loop(0, levels, finish, 0)

    def w_done(n, _):
        w_copy(lax.rem(e + n, ep)).wait_send()
        return 0

    lax.fori_loop(1, ep, w_done, 0)
    for k in range(3):
        out_copy(k).wait()


def per_device(tokens, cotangent, expert_ids, route_weight, gate_weight, up_weight, down_weight):
    ep, tp = lax.axis_size("ep"), lax.axis_size("tp")
    t_rows, width = tokens.shape
    _, f_rows, _ = gate_weight.shape
    levels = ep // 2
    span = width // tp
    slots = min(levels, 8)
    any_, vmem = pl.BlockSpec(memory_space=pl.ANY), pl.BlockSpec(memory_space=pltpu.VMEM)
    dma = pltpu.SemaphoreType.DMA
    big = jax.ShapeDtypeStruct((f_rows, width), BF16)
    scratch = [
        pltpu.VMEM((2, ep * t_rows, width), BF16),
        pltpu.VMEM((3, f_rows, width), BF16),
        pltpu.VMEM((ep, 1, t_rows), F32),
        pltpu.VMEM((ep, 1, t_rows), F32),
        pltpu.VMEM((slots, 2, t_rows, width), BF16),
        pltpu.VMEM((levels, t_rows, width), BF16),
        pltpu.VMEM((levels, 2, tp - 1, t_rows // 2, span), BF16),
        pltpu.VMEM((levels, t_rows, span), BF16),
        pltpu.VMEM((3, f_rows, ep * t_rows), BF16),
        pltpu.VMEM((3, f_rows, width), BF16),
        pltpu.VMEM((ep, 1, t_rows), F32),
        pltpu.VMEM((ep, 1, t_rows), F32),
        pltpu.VMEM((tp, ep, 1, t_rows), F32),
        dma((5,)), dma((ep,)), dma((ep,)), dma((2, 2, levels)), dma((2, levels)),
        dma((2, levels, 2, tp - 1)), dma((2, levels, 2, tp)), dma((2, levels)), dma((2, levels)),
        dma((levels,)), dma((levels,)), dma((levels, 2, tp - 1)), dma((levels, 2, tp - 1)),
        dma((levels,)), dma((levels,)), dma((ep,)), dma((ep,)), dma((tp,)), dma((tp,)), dma((3,)),
    ]
    dx, route, gate_grad, up_grad, down_grad = pl.pallas_call(
        functools.partial(kernel, ep, tp),
        out_shape=(
            jax.ShapeDtypeStruct((t_rows, span), BF16),
            jax.ShapeDtypeStruct(expert_ids.shape[::-1], F32), big, big, big),
        in_specs=[any_, any_, vmem, vmem, any_, any_, any_],
        out_specs=(vmem, vmem, any_, any_, any_),
        scratch_shapes=scratch,
        compiler_params=pltpu.CompilerParams(
            collective_id=0, has_side_effects=True, vmem_limit_bytes=66_000_000),
    )(tokens, cotangent, expert_ids.T, route_weight.T, gate_weight[0], up_weight[0], down_weight[0])
    wide = [g.astype(F32)[None] for g in (gate_grad, up_grad, down_grad)]
    return dx, route.T, *wide


def solution(mesh):
    in_specs = (
        P("ep", None), P("ep", None), P("ep", None), P("ep", None),
        P("ep", "tp", None), P("ep", "tp", None), P("ep", "tp", None),
    )
    out_specs = (
        P("ep", "tp"), P("ep", None), P("ep", "tp", None), P("ep", "tp", None), P("ep", "tp", None),
    )
    return jax.shard_map(
        per_device, mesh=mesh, in_specs=in_specs, out_specs=out_specs, check_vma=False
    )
```

profile of v0, /device:TPU:0, one launch (start us, length us, event | category | flops | bytes accessed | tf_op | source)
XLA Modules:
  0.0 80.3 jit_solution(11235282421655570597)
XLA Ops:
  0.6 72.7 %shard_map.110 = (bf16[128,512]{1,0:T(8,128)(2,1)}, f32[2,128]{1,0:T(2,128)}, bf16[256,2048]{1,0:T(8,128)(2,1)}, bf16[256,2048]{1,0:T(8,128)(2,1)}, bf16[256,2048]{1,0:T(8,128)(2,1)}) custom-call(bf16[128,2048]{1,0:T(8,128)(2,1)} %tokens.1, bf16[128,2048]{1,0:T(8,128)(2,1)} %cotangent.1, s32[2,128]{1,0:T(2,128)} %bitcast.18, bf16[2,128]{1,0:T(2,128)(2,1)} %bitcast.20, ...), custom_call_target="tpu_custom_call" | custom-call | tf_op jit(solution)/shard_map/pallas_call | solution.py:422
  73.3 0.0 copy-start
  73.3 4.2 %bitcast_convert_fusion = (f32[1,256,2048]{2,1,0:T(8,128)}, f32[1,256,2048]{2,1,0:T(8,128)}) fusion(bf16[256,2048]{1,0:T(8,128)(2,1)} %get-tuple-element.14, bf16[256,2048]{1,0:T(8,128)(2,1)} %get-tuple-element.13), kind=kLoop, calls=%fused_computation | loop fusion | flops 1048576 | bytes 6291456 | tf_op jit(solution)/shard_map/broadcast_in_dim | solution.py:433
  77.5 0.0 copy-start.1
  77.5 0.0 copy-start.2
  77.5 0.0 copy-done
  77.5 1.6 %bitcast_convert_fusion.2 = f32[1,256,2048]{2,1,0:T(8,128)} fusion(bf16[256,2048]{1,0:T(8,128)(2,1)S(1)} %copy-done), kind=kLoop, calls=%fused_computation.2 | loop fusion | flops 524288 | bytes 3145728 | tf_op jit(solution)/shard_map/broadcast_in_dim | solution.py:433
  79.1 0.0 copy-done.1
  79.1 0.7 copy.14
  79.7 0.0 copy-done.2
  79.7 0.6 copy.15
Async XLA Ops:
  73.3 4.2 %copy-start = (bf16[256,2048]{1,0:T(8,128)(2,1)S(1)}, bf16[256,2048]{1,0:T(8,128)(2,1)}, u32[]{:S(2)}) copy-start(bf16[256,2048]{1,0:T(8,128)(2,1)} %get-tuple-element.12) | copy-start | bytes 3145732
  77.5 1.6 %copy-start.1 = (bf16[128,512]{1,0:T(8,128)(2,1)S(1)}, bf16[128,512]{1,0:T(8,128)(2,1)}, u32[]{:S(2)}) copy-start(bf16[128,512]{1,0:T(8,128)(2,1)} %get-tuple-element.22) | copy-start | bytes 393220
  77.5 2.2 %copy-start.2 = (f32[2,128]{1,0:T(2,128)S(1)}, f32[2,128]{1,0:T(2,128)}, u32[]{:S(2)}) copy-start(f32[2,128]{1,0:T(2,128)} %get-tuple-element.11) | copy-start | bytes 3076
where the time goes:
time: 80.5 us; the launch traced here: 80.3 us
  Pallas kernels  72.7 us (90%)
  other arithmetic  5.72 us (7%)
  local copies, waits for them, and re-layouts  1.23 us (2%)
    pallas_call x1, Pallas kernels, per_device(): pl.pallas_call(functools.partial(kernel, ep, tp), out_shape=(jax.ShapeDty...  72.7 us
    broadcast_in_dim x2, other arithmetic, per_device(): wide = [g.astype(F32)[None] for g in (gate_grad, up_grad, down_grad)]  5.72 us

commit v1 on v0

--- a/solution.py
+++ b/solution.py
@@ -25,9 +25,9 @@
 def kernel(
     ep, tp, tokens, cotangent, ids, probs, gate_w, up_w, down_w,
     dx_out, route_out, gate_out, up_out, down_out,
-    rows, weights, pair_w, wg, part, core_in, tp_in, z_in, grads, totals, r_send, r_in, r_tp,
+    rows, weights, pair_w, wg, part, core_in, tp_in, z_in, grads, r_send, r_in, r_tp,
     load_sem, wz_send, wz_recv, z_send, z_recv, t_send, t_recv, c_send, c_recv,
-    pc_send, pc_recv, pt_send, pt_recv, pz_send, pz_recv, rs_send, rs_recv, rt_send, rt_recv, out_sem,
+    pc_send, pc_recv, pt_send, pt_recv, pz_send, pz_recv, rs_send, rs_recv, rt_send, rt_recv,
 ):
     e, j = lax.axis_index("ep"), lax.axis_index("tp")
     levels = ep // 2
@@ -273,20 +273,16 @@
 
     outs = (gate_out, up_out, down_out)
 
-    def out_copy(k):
-        return pltpu.make_async_copy(totals.at[k], outs[k], out_sem.at[k])
-
     def weight_grad(k):
         tile = min(width, 512)
 
         def column(n, _):
             cs = pl.ds(pl.multiple_of(n * tile, tile), tile)
-            totals[k, :, cs] = jnp.dot(
-                grads[k], rows[k // 2, :, cs], preferred_element_type=F32).astype(BF16)
+            outs[k][:, cs] = jnp.dot(
+                grads[k], rows[k // 2, :, cs], preferred_element_type=F32)
             return 0
 
         lax.fori_loop(0, width // tile, column, 0)
-        out_copy(k).start()
 
     compute(0)
     d_comp = nb + 1
@@ -386,8 +382,15 @@
         return 0
 
     lax.fori_loop(1, ep, w_done, 0)
-    for k in range(3):
-        out_copy(k).wait()
+
+
+def publish(*refs):
+    srcs, dsts, sem = refs[:5], refs[5:10], refs[10]
+    copies = [pltpu.make_async_copy(srcs[k], dsts[k], sem.at[k]) for k in (2, 3, 4, 0, 1)]
+    for copy in copies:
+        copy.start()
+    for copy in copies:
+        copy.wait()
 
 
 def per_device(tokens, cotangent, expert_ids, route_weight, gate_weight, up_weight, down_weight):
@@ -399,7 +402,7 @@
     slots = min(levels, 8)
     any_, vmem = pl.BlockSpec(memory_space=pl.ANY), pl.BlockSpec(memory_space=pltpu.VMEM)
     dma = pltpu.SemaphoreType.DMA
-    big = jax.ShapeDtypeStruct((f_rows, width), BF16)
+    big = pltpu.VMEM((f_rows, width), F32)
     scratch = [
         pltpu.VMEM((2, ep * t_rows, width), BF16),
         pltpu.VMEM((3, f_rows, width), BF16),
@@ -410,28 +413,35 @@
         pltpu.VMEM((levels, 2, tp - 1, t_rows // 2, span), BF16),
         pltpu.VMEM((levels, t_rows, span), BF16),
         pltpu.VMEM((3, f_rows, ep * t_rows), BF16),
-        pltpu.VMEM((3, f_rows, width), BF16),
         pltpu.VMEM((ep, 1, t_rows), F32),
         pltpu.VMEM((ep, 1, t_rows), F32),
         pltpu.VMEM((tp, ep, 1, t_rows), F32),
         dma((5,)), dma((ep,)), dma((ep,)), dma((2, 2, levels)), dma((2, levels)),
         dma((2, levels, 2, tp - 1)), dma((2, levels, 2, tp)), dma((2, levels)), dma((2, levels)),
         dma((levels,)), dma((levels,)), dma((levels, 2, tp - 1)), dma((levels, 2, tp - 1)),
-        dma((levels,)), dma((levels,)), dma((ep,)), dma((ep,)), dma((tp,)), dma((tp,)), dma((3,)),
+        dma((levels,)), dma((levels,)), dma((ep,)), dma((ep,)), dma((tp,)), dma((tp,)),
     ]
     dx, route, gate_grad, up_grad, down_grad = pl.pallas_call(
         functools.partial(kernel, ep, tp),
         out_shape=(
-            jax.ShapeDtypeStruct((t_rows, span), BF16),
-            jax.ShapeDtypeStruct(expert_ids.shape[::-1], F32), big, big, big),
+            pltpu.VMEM((t_rows, span), BF16),
+            pltpu.VMEM(expert_ids.shape[::-1], F32), big, big, big),
         in_specs=[any_, any_, vmem, vmem, any_, any_, any_],
-        out_specs=(vmem, vmem, any_, any_, any_),
+        out_specs=(vmem, vmem, vmem, vmem, vmem),
         scratch_shapes=scratch,
         compiler_params=pltpu.CompilerParams(
-            collective_id=0, has_side_effects=True, vmem_limit_bytes=66_000_000),
+            collective_id=0, has_side_effects=True, vmem_limit_bytes=66_900_000 - 12 * f_rows * width - 2 * t_rows * span),
     )(tokens, cotangent, expert_ids.T, route_weight.T, gate_weight[0], up_weight[0], down_weight[0])
-    wide = [g.astype(F32)[None] for g in (gate_grad, up_grad, down_grad)]
-    return dx, route.T, *wide
+    pieces = (dx, route, gate_grad, up_grad, down_grad)
+    dx, route, *wide = pl.pallas_call(
+        publish,
+        out_shape=tuple(jax.ShapeDtypeStruct(v.shape, v.dtype) for v in pieces),
+        in_specs=[vmem] * 5,
+        out_specs=(any_,) * 5,
+        scratch_shapes=[dma((5,))],
+        compiler_params=pltpu.CompilerParams(vmem_limit_bytes=1_000_000),
+    )(*(pltpu.with_memory_space_constraint(v, pltpu.VMEM) for v in pieces))
+    return dx, route.T, *(g[None] for g in wide)
 
 
 def solution(mesh):

time: 80.5 us -> 75.6 us (0.939)
  other arithmetic: 5.72 us -> 0 us
  Pallas kernels: 72.7 us -> 74.7 us
  local copies, waits for them, and re-layouts: 1.23 us -> 0 us
    broadcast_in_dim x2 -> x0, other arithmetic: 5.72 us -> none  [per_device(): wide = [g.astype(F32)[None] for g in (gate_grad, up_grad, down_grad)]]
    pallas_call x1 -> x2, Pallas kernels: 72.7 us -> 74.7 us  [the longest x1 72 us: per_device(): pl.pallas_call(functools.partial(kernel, ep, tp), out_shape=(pltpu.VMEM((...]
    unnamed x8 -> x0, local copies, waits for them, and re-layouts: 1.23 us -> none
where the time goes in v1:
time: 75.6 us; the launch traced here: 75.4 us
  Pallas kernels  74.7 us (99%)
    pallas_call x1, Pallas kernels, per_device(): pl.pallas_call(functools.partial(kernel, ep, tp), out_shape=(pltpu.VMEM((...  72 us
    pallas_call x1, Pallas kernels, per_device(): pl.pallas_call(publish, out_shape=tuple((jax.ShapeDtypeStruct(v.shape, v....  2.75 us

profile of v1, /device:TPU:0, one launch (start us, length us, event | category | flops | bytes accessed | tf_op | source)
XLA Modules:
  0.0 75.4 jit_solution(1350792363068835560)
XLA Ops:
  0.6 72.0 %shard_map.110 = (bf16[128,512]{1,0:T(8,128)(2,1)S(1)}, f32[2,128]{1,0:T(2,128)S(1)}, f32[256,2048]{1,0:T(8,128)S(1)}, f32[256,2048]{1,0:T(8,128)S(1)}, f32[256,2048]{1,0:T(8,128)S(1)}) custom-call(bf16[128,2048]{1,0:T(8,128)(2,1)} %tokens.1, bf16[128,2048]{1,0:T(8,128)(2,1)} %cotangent.1, s32[2,128]{1,0:T(2,128)} %bitcast.12, bf16[2,128]{1,0:T(2,128)(2,1)} %bitcast.13, ...), custom_call_target="tpu_custom_call" | custom-call | tf_op jit(solution)/shard_map/pallas_call | solution.py:424
  72.6 2.7 %shard_map.111 = (bf16[128,512]{1,0:T(8,128)(2,1)}, f32[2,128]{1,0:T(2,128)}, f32[256,2048]{1,0:T(8,128)}, f32[256,2048]{1,0:T(8,128)}, f32[256,2048]{1,0:T(8,128)}) custom-call(bf16[128,512]{1,0:T(8,128)(2,1)S(1)} %get-tuple-element.15.refs_0_, f32[2,128]{1,0:T(2,128)S(1)} %get-tuple-element.16.refs_1_, f32[256,2048]{1,0:T(8,128)S(1)} %get-tuple-element.17.refs_2_, ...), custom_call_target="tpu_custom_call" | custom-call | tf_op jit(solution)/shard_map/pallas_call | solution.py:436

commit v2 on v1

v2 whole, which is shorter than its diff:
```python
import functools

import jax
import jax.numpy as jnp
from jax import lax
from jax.experimental import pallas as pl
from jax.experimental.pallas import tpu as pltpu
from jax.sharding import PartitionSpec as P

MESH = pl.DeviceIdType.MESH
F32 = jnp.float32
BF16 = jnp.bfloat16
NT = (((1,), (1,)), ((), ()))
TN = (((0,), (0,)), ((), ()))
VMEM_BYTES = 66_900_000
AHEAD = 1


def slices_for(j, bits, count):
    base = j
    for bit in bits:
        base = base - ((j // bit) % 2) * bit
    out = []
    for k in range(count):
        out.append(base + sum(bit for n, bit in enumerate(bits) if (k >> n) & 1))
    return out


def kernel(
    ep, tp, cap, tokens, cotangent, ids_in, probs_in, gate_w, up_w, down_w,
    dx_out, route_out, gate_out, up_out, down_out,
    ids, probs, xin, hot, hot_t, stage, mate_rows, whole, rows, weights, pw_out, pw_in, grads, part, ta_in, tb_in, z_in,
    r_send, r_in, r_tp, r_mat,
    load_sem, z_send, z_recv, m_send, m_recv, f_send, f_recv, w_send, w_recv, ta_send, ta_recv, tb_send, tb_recv,
    pa_send, pa_recv, pb_send, pb_recv, pz_send, pz_recv, rs_send, rs_recv, rt_send, rt_recv,
):
    e, j = lax.axis_index("ep"), lax.axis_index("tp")
    levels = ep // 2
    lvl, core = e // 2, e % 2
    mate = e + 1 - 2 * core
    t_rows, width = tokens.shape
    span = width // tp
    half = cap // 2
    nb = tp.bit_length() - 1
    lb = levels.bit_length() - 1
    far = 2 * (levels - 1)
    units = far + 2
    tile = min(width, 512)

    def xor(a, b):
        out = 0
        for n in range(lb):
            p, q = (a // (1 << n)) % 2, (b // (1 << n)) % 2
            out = out + (p + q - 2 * p * q) * (1 << n)
        return out

    def level_of(u):
        d = u // 2 + 1 + u % 2
        return xor(lvl, jnp.where(d >= levels, 1, d))

    def source(v):
        u = jnp.maximum(v - 2, 0)
        return jnp.where(v == 0, e, jnp.where(v == 1, mate, 2 * level_of(u) + u % 2))

    def blk(s):
        return pl.ds(pl.multiple_of(s * cap, cap), cap)

    def col(s):
        return pl.ds(pl.multiple_of(s * span, span), span)

    def run(first, count):
        return pl.ds(pl.multiple_of(first * span, span), count * span)

    def flip(bit):
        return j + bit * (1 - 2 * ((j // bit) % 2))

    def remote(src, dst, ssem, rsem, de, dt):
        return pltpu.make_async_remote_copy(
            src_ref=src, dst_ref=dst, send_sem=ssem, recv_sem=rsem,
            device_id=(de, dt), device_id_type=MESH)

    small = [
        pltpu.make_async_copy(ids_in, ids, load_sem.at[5]),
        pltpu.make_async_copy(probs_in, probs, load_sem.at[6]),
    ]
    loads = [
        pltpu.make_async_copy(tokens, xin.at[0], load_sem.at[0]),
        pltpu.make_async_copy(cotangent, xin.at[1], load_sem.at[1]),
        pltpu.make_async_copy(gate_w, weights.at[0], load_sem.at[2]),
        pltpu.make_async_copy(up_w, weights.at[1], load_sem.at[3]),
        pltpu.make_async_copy(down_w, weights.at[2], load_sem.at[4]),
    ]
    for copy in small + loads:
        copy.start()
    barrier = pltpu.get_barrier_semaphore()

    def greet(n, _):
        pl.semaphore_signal(barrier, inc=1, device_id=(lax.rem(e + n, ep), j), device_id_type=MESH)
        return 0

    def greet_tp(n, _):
        pl.semaphore_signal(barrier, inc=1, device_id=(e, lax.rem(j + n, tp)), device_id_type=MESH)
        return 0

    lax.fori_loop(1, ep, greet, 0)
    lax.fori_loop(1, tp, greet_tp, 0)

    def z_copy(a, d):
        return remote(stage.at[a, blk(d)], rows.at[a, blk(e), col(j)],
                      z_send.at[a, d], z_recv.at[a, e], d, j)

    def z_wait(a, s):
        return remote(stage.at[a, blk(s)], rows.at[a, blk(s), col(j)],
                      z_send.at[a, s], z_recv.at[a, s], s, j)

    def m_copy(a, s):
        return remote(mate_rows.at[a], rows.at[a, blk(s)], m_send.at[a], m_recv.at[a], mate, j)

    def full_copy(a, c, s, d):
        return remote(whole.at[a, c], rows.at[a, blk(s)], f_send.at[a, c], f_recv.at[a], d, j)

    def w_copy(d, s):
        return remote(pw_out.at[d], pw_in.at[s], w_send.at[d], w_recv.at[s], d, j)

    def gather_step(a, s, n, receive):
        peer = flip(1 << n if a == 0 else tp >> (n + 1))
        owner = peer if receive else j
        if a == 0:
            ref = rows.at[a, blk(s), run(owner - owner % (1 << n), 1 << n)]
            return [remote(ref, ref, ta_send.at[s, n], ta_recv.at[s, n], e, peer)]
        copies = []
        for k, sid in enumerate(slices_for(owner, [tp >> (i + 1) for i in range(n)], 1 << n)):
            ref = rows.at[a, blk(s), col(sid)]
            at = (1 << n) - 1 + k
            copies.append(remote(ref, ref, tb_send.at[s, at], tb_recv.at[s, at], e, peer))
        return copies

    def scatter_step(s, n, receive):
        base, count = tp - (tp >> n), tp >> (n + 1)
        copies = []
        peer = flip(1 << n)
        owner = j if receive else peer
        for k, sid in enumerate(slices_for(owner, [1 << i for i in range(n + 1, nb)], count)):
            src, dst, at = part.at[s, :half, col(sid)], tb_in.at[s, base + k], base + k
            copies.append((remote(src, dst, pb_send.at[s, at], pb_recv.at[s, at], e, peer), src, dst))
        peer = flip(count)
        owner = j if receive else peer
        src = part.at[s, half:, run(owner - owner % count, count)]
        dst = ta_in.at[s, :, base * span:(base + count) * span]
        copies.append((remote(src, dst, pa_send.at[s, n], pa_recv.at[s, n], e, peer), src, dst))
        return copies

    def pz_copy(d, s):
        return remote(part.at[d, :, col(j)], z_in.at[blk(s)], pz_send.at[d], pz_recv.at[s], d, j)

    def r_copy(d, s):
        return remote(r_send.at[d], r_in.at[s], rs_send.at[d], rs_recv.at[s], d, j)

    def send(u, arrays):
        l = level_of(u)
        for a in arrays:
            for c in range(2):
                z_copy(a, 2 * l + c).start()

    for copy in small:
        copy.wait()
    idr = ids[...]
    lane_e = lax.broadcasted_iota(jnp.int32, (ep, t_rows), 0)
    first, second = lane_e == idr[0:1], lane_e == idr[1:2]
    mask = jnp.where(first | second, 1.0, 0.0)
    before = jnp.where(
        lax.broadcasted_iota(jnp.int32, (t_rows, t_rows), 0)
        < lax.broadcasted_iota(jnp.int32, (t_rows, t_rows), 1), 1.0, 0.0).astype(BF16)
    rank = jnp.dot(mask.astype(BF16), before, preferred_element_type=F32)
    key = jnp.where(mask > 0.0, rank, -1.0)
    slot = lax.broadcasted_iota(jnp.int32, (cap, t_rows), 0).astype(F32)
    for x in range(ep):
        hot[x * cap:(x + 1) * cap] = jnp.where(key[x:x + 1] == slot, 1.0, 0.0).astype(BF16)

    def select(a):
        stage[a] = jnp.dot(
            hot[...], xin[a, :, col(j)], preferred_element_type=F32).astype(BF16)

    loads[0].wait()
    select(0)
    pl.semaphore_wait(barrier, ep + tp - 2)
    if far:
        send(core, (0,))
    loads[1].wait()
    select(1)
    if far:
        send(core, (1,))

    p = probs[...].astype(F32)
    chosen = (jnp.where(first, p[0:1], 0.0) + jnp.where(second, p[1:2], 0.0)).astype(BF16)
    slot_p = lax.dot_general(chosen, hot[...], NT, preferred_element_type=F32)
    for x in range(ep):
        pw_out[x, :, :cap] = slot_p[x:x + 1, x * cap:(x + 1) * cap]

    def w_start(n, _):
        w_copy(lax.rem(e + n, ep), e).start()
        return 0

    lax.fori_loop(1, ep, w_start, 0)
    pw_in[e] = pw_out[e]

    for a in range(2):
        for n in range(width // tile):
            cs = pl.ds(n * tile, tile)
            mate_rows[a, :, cs] = jnp.dot(
                hot[blk(mate)], xin[a, :, cs], preferred_element_type=F32).astype(BF16)
        m_copy(a, e).start()
    for a in range(2):
        for n in range(width // tile):
            cs = pl.ds(n * tile, tile)
            rows[a, blk(e), cs] = jnp.dot(
                hot[blk(e)], xin[a, :, cs], preferred_element_type=F32).astype(BF16)
    for n in range(2, 5):
        loads[n].wait()

    def arrive(u):
        s = source(u + 2)
        for a in range(2):
            z_wait(a, s).wait_recv()
            for copy in gather_step(a, s, 0, False):
                copy.start()

    def spread(u, n):
        s = source(u + 2)
        for a in range(2):
            for copy in gather_step(a, s, n - 1, True):
                copy.wait_recv()
            for copy in gather_step(a, s, n, False):
                copy.start()

    def feed(u):
        @pl.when(core == u % 2)
        def _():
            send(u, (0, 1))

    def feed_whole():
        near = 2 * level_of(far - 1)
        for a in range(2):
            for c in range(2):
                for n in range(width // tile):
                    cs = pl.ds(n * tile, tile)
                    whole[a, c, :, cs] = jnp.dot(
                        hot[blk(near + c)], xin[a, :, cs], preferred_element_type=F32).astype(BF16)
                full_copy(a, c, e, near + c).start()

    def compute(v):
        s = source(v)
        @pl.when(v == 1)
        def _():
            for a in range(2):
                m_copy(a, mate).wait_recv()
        if far:
            @pl.when(v == units - 1)
            def _():
                for a in range(2):
                    full_copy(a, 0, s, s).wait_recv()
        @pl.when(jnp.logical_and(v >= 2, v < units - 1))
        def _():
            for a in range(2):
                for copy in gather_step(a, s, nb - 1, True):
                    copy.wait_recv()
        @pl.when(v >= 1)
        def _():
            w_copy(s, s).wait_recv()
        x = rows[0, blk(s), :]
        pre_gate = lax.dot_general(x, weights[0], NT, preferred_element_type=F32)
        pre_up = lax.dot_general(x, weights[1], NT, preferred_element_type=F32)
        back = lax.dot_general(rows[1, blk(s), :], weights[2], NT, preferred_element_type=F32)
        p = jnp.broadcast_to(pw_in[s], (8, t_rows)).T[:cap, 0:1]
        sigma = jax.nn.sigmoid(pre_gate)
        silu = pre_gate * sigma
        hidden = silu * pre_up
        scaled = p * back
        gg = (scaled * pre_up * sigma * (1.0 + pre_gate * (1.0 - sigma))).astype(BF16)
        gu = (scaled * silu).astype(BF16)
        for n in range(width // tile):
            cs = pl.ds(n * tile, tile)
            part[s, :, cs] = (
                jnp.dot(gg, weights[0, :, cs], preferred_element_type=F32)
                + jnp.dot(gu, weights[1, :, cs], preferred_element_type=F32)).astype(BF16)
        for copy, _, _ in scatter_step(s, 0, False):
            copy.start()
        grads[0, blk(s)] = gg
        grads[1, blk(s)] = gu
        grads[2, blk(s)] = (p * hidden).astype(BF16)
        prod = jnp.sum(hidden * back, axis=1, keepdims=True)
        r_send[s, :, :cap] = jnp.broadcast_to(prod, (cap, t_rows)).T[0:1]
        @pl.when(v >= 1)
        def _():
            r_copy(s, e).start()
        @pl.when(v == 0)
        def _():
            r_in[e] = r_send[e]

    def merge(v, n):
        s = source(v)
        for (copy, _, _), (_, mine, got) in zip(scatter_step(s, n, False), scatter_step(s, n, True)):
            copy.wait()
            mine[...] = (mine[...].astype(F32) + got[...].astype(F32)).astype(BF16)
        if n + 1 < nb:
            for copy, _, _ in scatter_step(s, n + 1, False):
                copy.start()
        else:
            @pl.when(v >= 1)
            def _():
                pz_copy(s, e).start()
            @pl.when(v == 0)
            def _():
                z_in[blk(e)] = part[e, :, col(j)]

    outs = (gate_out, up_out, down_out)

    def weight_grad(k):
        left = grads[k].T
        for n in range(width // tile):
            cs = pl.ds(n * tile, tile)
            outs[k][:, cs] = jnp.dot(left, rows[k // 2, :, cs], preferred_element_type=F32)

    begin = nb + AHEAD + 1
    last = units - 2 + begin

    def tick(t, _):
        def stage_of(f, i, low, high):
            @pl.when(jnp.logical_and(i >= low, i < high))
            def _():
                f(i)

        stage_of(compute, jnp.where(t < 2, t, jnp.where(t >= begin, t - begin + 2, -1)), 0, units)
        if far:
            stage_of(feed, jnp.where(t == 1, 2, jnp.where(t > 2, t, 0)), 2, far - 1)
            @pl.when(jnp.logical_and(t == max(1, far - 3), core == 1))
            def _():
                feed_whole()
            stage_of(arrive, t - 1, 0, far - 1)
            for n in range(1, nb):
                stage_of(functools.partial(spread, n=n), t - 1 - n, 0, far - 1)
        @pl.when(t == last)
        def _():
            weight_grad(0)
        @pl.when(t == last + 1)
        def _():
            lax.fori_loop(1, ep, r_wait, 0)
            lax.fori_loop(1, tp, rt_start, 0)
            r_tp[j] = r_in[...]
            weight_grad(1)
        for n in range(nb - 1, -1, -1):
            own, other = t - 1 - n, t - begin - 1 - n + 2
            stage_of(functools.partial(merge, n=n), jnp.where(
                own < 2, own, jnp.where(other >= 2, other, -1)), 0, units)
        return 0

    def r_wait(n, _):
        s = lax.rem(e + n, ep)
        r_copy(s, s).wait()
        return 0

    def rt_copy(d, s):
        return remote(r_in, r_tp.at[s], rt_send.at[d], rt_recv.at[s], e, d)

    def rt_start(n, _):
        rt_copy(lax.rem(j + n, tp), j).start()
        return 0

    def rt_wait(n, _):
        s = lax.rem(j + n, tp)
        rt_copy(s, s).wait()
        return 0

    lax.fori_loop(0, last + nb + 1, tick, 0)
    weight_grad(2)
    hot_t[...] = hot[...].T
    lax.fori_loop(1, tp, rt_wait, 0)
    for x in range(ep):
        total = r_tp[0, x]
        for i in range(1, tp):
            total = total + r_tp[i, x]
        r_mat[x:x + 1, :cap] = total[:, :cap]
    sums = r_mat[...].T
    found = [jnp.zeros((1, t_rows), F32) for _ in range(2)]
    for x in range(ep):
        value = jnp.sum(
            hot[x * cap:(x + 1) * cap].astype(F32) * sums[:cap, x:x + 1], axis=0, keepdims=True)
        found = [f + jnp.where(idr[k:k + 1] == x, value, 0.0) for k, f in enumerate(found)]
    for k in range(2):
        route_out[k:k + 1] = found[k]

    def pz_wait(n, _):
        s = lax.rem(e + n, ep)
        pz_copy(s, s).wait()
        return 0

    lax.fori_loop(1, ep, pz_wait, 0)
    dx_out[...] = jnp.dot(hot_t[...], z_in[...], preferred_element_type=F32).astype(BF16)
    def finish(n, _):
        d = lax.rem(e + n, ep)
        w_copy(d, e).wait_send()
        if far:
            @pl.when(jnp.logical_and(d // 2 != lvl, jnp.logical_or(core == 0, d // 2 != level_of(far - 1))))
            def _():
                for a in range(2):
                    z_copy(a, d).wait_send()
            @pl.when(jnp.logical_and(d // 2 != lvl, d != 2 * level_of(far - 1) + 1))
            def _():
                for a in range(2):
                    for i in range(nb):
                        for copy in gather_step(a, d, i, False):
                            copy.wait_send()
        return 0

    if far:
        @pl.when(core == 1)
        def _():
            for a in range(2):
                for c in range(2):
                    full_copy(a, c, e, 2 * level_of(far - 1) + c).wait_send()
    lax.fori_loop(1, ep, finish, 0)
    for a in range(2):
        m_copy(a, e).wait_send()


def publish(*refs):
    srcs, dsts, sem = refs[:5], refs[5:10], refs[10]
    copies = [pltpu.make_async_copy(srcs[k], dsts[k], sem.at[k]) for k in (2, 3, 4, 0, 1)]
    for copy in copies:
        copy.start()
    for copy in copies:
        copy.wait()


def per_device(tokens, cotangent, expert_ids, route_weight, gate_weight, up_weight, down_weight):
    ep, tp = lax.axis_size("ep"), lax.axis_size("tp")
    t_rows, width = tokens.shape
    top = expert_ids.shape[1]
    _, f_rows, _ = gate_weight.shape
    cap = min(t_rows, 2 * top * t_rows // ep)
    span = width // tp
    nb = tp.bit_length() - 1
    any_, vmem = pl.BlockSpec(memory_space=pl.ANY), pl.BlockSpec(memory_space=pltpu.VMEM)
    dma = pltpu.SemaphoreType.DMA
    big = pltpu.VMEM((f_rows, width), F32)
    scratch = [
        pltpu.VMEM(expert_ids.shape[::-1], jnp.int32),
        pltpu.VMEM(route_weight.shape[::-1], route_weight.dtype),
        pltpu.VMEM((2, t_rows, width), BF16),
        pltpu.VMEM((ep * cap, t_rows), BF16),
        pltpu.VMEM((t_rows, ep * cap), BF16),
        pltpu.VMEM((2, ep * cap, span), BF16),
        pltpu.VMEM((2, cap, width), BF16),
        pltpu.VMEM((2, 2, cap, width), BF16),
        pltpu.VMEM((2, ep * cap, width), BF16),
        pltpu.VMEM((3, f_rows, width), BF16),
        pltpu.VMEM((ep, 1, t_rows), F32),
        pltpu.VMEM((ep, 1, t_rows), F32),
        pltpu.VMEM((3, ep * cap, f_rows), BF16),
        pltpu.VMEM((ep, cap, width), BF16),
        pltpu.VMEM((ep, cap // 2, (tp - 1) * span), BF16),
        pltpu.VMEM((ep, tp - 1, cap // 2, span), BF16),
        pltpu.VMEM((ep * cap, span), BF16),
        pltpu.VMEM((ep, 1, t_rows), F32),
        pltpu.VMEM((ep, 1, t_rows), F32),
        pltpu.VMEM((tp, ep, 1, t_rows), F32),
        pltpu.VMEM((ep, t_rows), F32),
        dma((7,)), dma((2, ep)), dma((2, ep)), dma((2,)), dma((2,)), dma((2, 2)), dma((2,)), dma((ep,)), dma((ep,)),
        dma((ep, nb)), dma((ep, nb)), dma((ep, tp - 1)), dma((ep, tp - 1)),
        dma((ep, nb)), dma((ep, nb)), dma((ep, tp - 1)), dma((ep, tp - 1)),
        dma((ep,)), dma((ep,)), dma((ep,)), dma((ep,)), dma((tp,)), dma((tp,)),
    ]
    pieces = pl.pallas_call(
        functools.partial(kernel, ep, tp, cap),
        out_shape=(
            pltpu.VMEM((t_rows, span), BF16),
            pltpu.VMEM(expert_ids.shape[::-1], F32), big, big, big),
        in_specs=[any_] * 7,
        out_specs=(vmem,) * 5,
        scratch_shapes=scratch,
        compiler_params=pltpu.CompilerParams(
            collective_id=0, has_side_effects=True,
            vmem_limit_bytes=VMEM_BYTES - 12 * f_rows * width - 2 * t_rows * span),
    )(tokens, cotangent, expert_ids.T, route_weight.T, gate_weight[0], up_weight[0], down_weight[0])
    dx, route, *wide = pl.pallas_call(
        publish,
        out_shape=tuple(jax.ShapeDtypeStruct(v.shape, v.dtype) for v in pieces),
        in_specs=[vmem] * 5,
        out_specs=(any_,) * 5,
        scratch_shapes=[dma((5,))],
        compiler_params=pltpu.CompilerParams(vmem_limit_bytes=1_000_000),
    )(*(pltpu.with_memory_space_constraint(v, pltpu.VMEM) for v in pieces))
    return dx, route.T, *(g[None] for g in wide)


def solution(mesh):
    in_specs = (
        P("ep", None), P("ep", None), P("ep", None), P("ep", None),
        P("ep", "tp", None), P("ep", "tp", None), P("ep", "tp", None),
    )
    out_specs = (
        P("ep", "tp"), P("ep", None), P("ep", "tp", None), P("ep", "tp", None), P("ep", "tp", None),
    )
    return jax.shard_map(
        per_device, mesh=mesh, in_specs=in_specs, out_specs=out_specs, check_vma=False
    )
```

time: 75.6 us -> 65.1 us (0.86)
  Pallas kernels: 74.7 us -> 63.7 us
    pallas_call x1, Pallas kernels: 72 us -> 60.9 us  [per_device(): pl.pallas_call(functools.partial(kernel, ep, tp, cap), out_shape=(pltpu.V...]
where the time goes in v2:
time: 65.1 us; the launch traced here: 64.3 us
  Pallas kernels  63.7 us (98%)
    pallas_call x1, Pallas kernels, per_device(): pl.pallas_call(functools.partial(kernel, ep, tp, cap), out_shape=(pltpu.V...  60.9 us
    pallas_call x1, Pallas kernels, per_device(): pl.pallas_call(publish, out_shape=tuple((jax.ShapeDtypeStruct(v.shape, v....  2.75 us

profile of v2, /device:TPU:0, one launch (start us, length us, event | category | flops | bytes accessed | tf_op | source)
XLA Modules:
  0.0 64.3 jit_solution(8387067386532410634)
XLA Ops:
  0.6 60.9 %shard_map.110 = (bf16[128,512]{1,0:T(8,128)(2,1)S(1)}, f32[2,128]{1,0:T(2,128)S(1)}, f32[256,2048]{1,0:T(8,128)S(1)}, f32[256,2048]{1,0:T(8,128)S(1)}, f32[256,2048]{1,0:T(8,128)S(1)}) custom-call(bf16[128,2048]{1,0:T(8,128)(2,1)} %tokens.1, bf16[128,2048]{1,0:T(8,128)(2,1)} %cotangent.1, s32[2,128]{1,0:T(2,128)} %bitcast.12, bf16[2,128]{1,0:T(2,128)(2,1)} %bitcast.13, ...), custom_call_target="tpu_custom_call" | custom-call | tf_op jit(solution)/shard_map/pallas_call | solution.py:473
  61.6 2.7 %shard_map.111 = (bf16[128,512]{1,0:T(8,128)(2,1)}, f32[2,128]{1,0:T(2,128)}, f32[256,2048]{1,0:T(8,128)}, f32[256,2048]{1,0:T(8,128)}, f32[256,2048]{1,0:T(8,128)}) custom-call(bf16[128,512]{1,0:T(8,128)(2,1)S(1)} %get-tuple-element.15.refs_0_, f32[2,128]{1,0:T(2,128)S(1)} %get-tuple-element.16.refs_1_, f32[256,2048]{1,0:T(8,128)S(1)} %get-tuple-element.17.refs_2_, ...), custom_call_target="tpu_custom_call" | custom-call | tf_op jit(solution)/shard_map/pallas_call | solution.py:485

commit v3 on v2

v3 whole, which is shorter than its diff:
```python
import functools

import jax
import jax.numpy as jnp
from jax import lax
from jax.experimental import pallas as pl
from jax.experimental.pallas import tpu as pltpu
from jax.sharding import PartitionSpec as P

MESH = pl.DeviceIdType.MESH
F32 = jnp.float32
BF16 = jnp.bfloat16
NT = (((1,), (1,)), ((), ()))
TN = (((0,), (0,)), ((), ()))
VMEM_BYTES = 66_900_000


def slices_for(j, bits, count):
    base = j
    for bit in bits:
        base = base - ((j // bit) % 2) * bit
    out = []
    for k in range(count):
        out.append(base + sum(bit for n, bit in enumerate(bits) if (k >> n) & 1))
    return out


def kernel(
    ep, tp, cap, tokens, cotangent, ids_in, probs_in, gate_w, up_w, down_w,
    dx_out, route_out, gate_out, up_out, down_out,
    ids, probs, xin, hot, hot_t, stage, mate_rows, whole, diag, rows, weights, pw_out, pw_in, grads, part, ta_in, tb_in, z_in,
    r_send, r_in, r_tp, r_mat,
    load_sem, z_send, z_recv, m_send, m_recv, f_send, f_recv, x_send, x_recv, d_send, d_recv,
    w_send, w_recv, t_send, t_recv, p_send, p_recv, pz_send, pz_recv, rs_send, rs_recv,
    rt_send, rt_recv,
):
    e, j = lax.axis_index("ep"), lax.axis_index("tp")
    levels = ep // 2
    lvl, core = e // 2, e % 2
    mate = e + 1 - 2 * core
    t_rows, width = tokens.shape
    span = width // tp
    half = cap // 2
    nb = tp.bit_length() - 1
    lb = levels.bit_length() - 1
    far = 2 * (levels - 1)
    units = far + 2
    crossed = False
    first_spread = 1 if crossed else 0
    spread_end = far - 1
    spreads = spread_end - first_spread
    tile = min(width, 512)

    def xor(a, b):
        out = 0
        for n in range(lb):
            p, q = (a // (1 << n)) % 2, (b // (1 << n)) % 2
            out = out + (p + q - 2 * p * q) * (1 << n)
        return out

    def level_of(u):
        d = u // 2 + 1 + u % 2
        return xor(lvl, jnp.where(d >= levels, 1, d))

    def source(w):
        v = jnp.where(w == units - 2, units - 1, jnp.where(w == units - 1, units - 2, w)) if far else w
        u = jnp.maximum(v - 2, 0)
        return jnp.where(v == 0, e, jnp.where(v == 1, mate, 2 * level_of(u) + u % 2))

    def blk(s):
        return pl.ds(pl.multiple_of(s * cap, cap), cap)

    def col(s):
        return pl.ds(pl.multiple_of(s * span, span), span)

    def run(first, count):
        return pl.ds(pl.multiple_of(first * span, span), count * span)

    def flip(bit):
        return j + bit * (1 - 2 * ((j // bit) % 2))

    def remote(src, dst, ssem, rsem, de, dt):
        return pltpu.make_async_remote_copy(
            src_ref=src, dst_ref=dst, send_sem=ssem, recv_sem=rsem,
            device_id=(de, dt), device_id_type=MESH)

    small = [
        pltpu.make_async_copy(ids_in, ids, load_sem.at[5]),
        pltpu.make_async_copy(probs_in, probs, load_sem.at[6]),
    ]
    loads = [
        pltpu.make_async_copy(tokens, xin.at[0], load_sem.at[0]),
        pltpu.make_async_copy(cotangent, xin.at[1], load_sem.at[1]),
        pltpu.make_async_copy(gate_w, weights.at[0], load_sem.at[2]),
        pltpu.make_async_copy(up_w, weights.at[1], load_sem.at[3]),
        pltpu.make_async_copy(down_w, weights.at[2], load_sem.at[4]),
    ]
    for copy in small + loads:
        copy.start()
    barrier = pltpu.get_barrier_semaphore()

    def greet(n, _):
        pl.semaphore_signal(barrier, inc=1, device_id=(lax.rem(e + n, ep), j), device_id_type=MESH)
        return 0

    def greet_tp(n, _):
        pl.semaphore_signal(barrier, inc=1, device_id=(e, lax.rem(j + n, tp)), device_id_type=MESH)
        return 0

    lax.fori_loop(1, ep, greet, 0)
    lax.fori_loop(1, tp, greet_tp, 0)

    def z_copy(a, u, d):
        return remote(stage.at[a, blk(d)], rows.at[a, blk(e), col(j)],
                      z_send, z_recv.at[a, u], d, j)

    def z_wait(a, u, s):
        return remote(stage.at[a, blk(s)], rows.at[a, blk(s), col(j)],
                      z_send, z_recv.at[a, u], s, j)

    def m_copy(s):
        return remote(mate_rows, rows.at[:, blk(s)], m_send, m_recv, mate, j)

    def full_copy(c, s, d):
        return remote(whole.at[c], rows.at[:, blk(s)], f_send, f_recv, d, j)

    def cross_copy(bit, s, receive):
        peer = flip(bit)
        ref = rows.at[:, blk(s), col(peer if receive else j)]
        return remote(ref, ref, x_send, x_recv.at[bit - 1], e, peer)

    def diag_copy(c, s, d):
        return remote(diag.at[c], rows.at[:, blk(s), col(tp - 1 - j)], d_send, d_recv, d, j)

    def w_copy(d, s):
        return remote(pw_out.at[d], pw_in.at[s], w_send, w_recv.at[0], d, j)

    def w_mate(s):
        return remote(pw_out.at[mate], pw_in.at[s], w_send, w_recv.at[1], mate, j)

    def gather_step(a, u, s, n):
        peer = flip(1 << n if a == 0 else tp >> (n + 1))
        if a == 0:
            ref = rows.at[a, blk(s), run(j - j % (1 << n), 1 << n)]
            return [remote(ref, ref, t_send, t_recv.at[a, u, n], e, peer)]
        copies = []
        for sid in slices_for(j, [tp >> (i + 1) for i in range(n)], 1 << n):
            ref = rows.at[a, blk(s), col(sid)]
            copies.append(remote(ref, ref, t_send, t_recv.at[a, u, n], e, peer))
        return copies

    def gather_wait(a, u, s, n):
        ref = rows.at[a, blk(s), run(0, 1 << n)]
        remote(ref, ref, t_send, t_recv.at[a, u, n], e, flip(1)).wait_recv()

    def scatter_step(w, s, n):
        base, count = tp - (tp >> n), tp >> (n + 1)
        copies = []
        for k in range(count):
            peer = flip(1 << n)
            bits = [1 << i for i in range(n + 1, nb)]
            mine = part.at[s, :half, col(slices_for(j, bits, count)[k])]
            src = part.at[s, :half, col(slices_for(peer, bits, count)[k])]
            got = tb_in.at[s, base + k]
            copies.append((remote(src, got, p_send, p_recv.at[w, n], e, peer), mine, got))
        peer = flip(count)
        mine = part.at[s, half:, run(j - j % count, count)]
        src = part.at[s, half:, run(peer - peer % count, count)]
        got = ta_in.at[s, :, base * span:(base + count) * span]
        copies.append((remote(src, got, p_send, p_recv.at[w, n], e, peer), mine, got))
        return copies

    def scatter_wait(w, n):
        ref = part.at[0, :, run(0, tp >> (n + 1))]
        remote(ref, ref, p_send, p_recv.at[w, n], e, flip(1)).wait_recv()

    def pz_copy(d, s):
        return remote(part.at[d, :, col(j)], z_in.at[blk(s)], pz_send, pz_recv, d, j)

    def r_copy(d, s):
        return remote(r_send.at[d], r_in.at[s], rs_send, rs_recv, d, j)

    def send(u, arrays):
        l = level_of(u)
        for a in arrays:
            for c in range(2):
                z_copy(a, u, 2 * l + c).start()

    for copy in small:
        copy.wait()
    idr = ids[...]
    lane_e = lax.broadcasted_iota(jnp.int32, (ep, t_rows), 0)
    first, second = lane_e == idr[0:1], lane_e == idr[1:2]
    mask = jnp.where(first | second, 1.0, 0.0)
    before = jnp.where(
        lax.broadcasted_iota(jnp.int32, (t_rows, t_rows), 0)
        < lax.broadcasted_iota(jnp.int32, (t_rows, t_rows), 1), 1.0, 0.0).astype(BF16)
    rank = jnp.dot(mask.astype(BF16), before, preferred_element_type=F32)
    key = jnp.where(mask > 0.0, rank, -1.0)
    slot = lax.broadcasted_iota(jnp.int32, (cap, t_rows), 0).astype(F32)
    for x in range(ep):
        hot[x * cap:(x + 1) * cap] = jnp.where(key[x:x + 1] == slot, 1.0, 0.0).astype(BF16)

    def select(a):
        stage[a] = jnp.dot(
            hot[...], xin[a, :, col(j)], preferred_element_type=F32).astype(BF16)

    for a in range(2):
        loads[a].wait()
        select(a)
        for n in range(width // tile):
            cs = pl.ds(n * tile, tile)
            mate_rows[a, :, cs] = jnp.dot(
                hot[blk(mate)], xin[a, :, cs], preferred_element_type=F32).astype(BF16)
            rows[a, blk(e), cs] = jnp.dot(
                hot[blk(e)], xin[a, :, cs], preferred_element_type=F32).astype(BF16)

    p = probs[...].astype(F32)
    chosen = (jnp.where(first, p[0:1], 0.0) + jnp.where(second, p[1:2], 0.0)).astype(BF16)
    slot_p = lax.dot_general(chosen, hot[...], NT, preferred_element_type=F32)
    for x in range(ep):
        pw_out[x, :, :cap] = slot_p[x:x + 1, x * cap:(x + 1) * cap]
    pw_in[e] = pw_out[e]

    def w_start(n, _):
        d = lax.rem(e + n, ep)
        @pl.when(d != mate)
        def _():
            w_copy(d, e).start()
        return 0

    pl.semaphore_wait(barrier, ep + tp - 2)
    lax.fori_loop(1, ep, w_start, 0)
    w_mate(e).start()
    if far:
        send(core, (0, 1))
    m_copy(e).start()
    if crossed:
        @pl.when(core == 0)
        def _():
            for a in range(2):
                for c in range(2):
                    diag[c, a] = jnp.dot(
                        hot[blk(2 * level_of(0) + c)], xin[a, :, col(tp - 1 - j)],
                        preferred_element_type=F32).astype(BF16)
            for c in range(2):
                diag_copy(c, e, 2 * level_of(0) + c).start()
    for n in range(2, 5):
        loads[n].wait()

    def source_of(u):
        return 2 * level_of(u) + u % 2

    def arrive(u):
        s = source_of(u)
        for a in range(2):
            z_wait(a, u, s).wait_recv()
            @pl.when(u >= first_spread)
            def _():
                for copy in gather_step(a, u, s, 0):
                    copy.start()
        if crossed:
            @pl.when(u == 0)
            def _():
                for bit in (1, 2):
                    cross_copy(bit, s, False).start()

    def spread(u, n):
        s = source_of(u)
        for a in range(2):
            gather_wait(a, u, s, n - 1)
            for copy in gather_step(a, u, s, n):
                copy.start()

    def feed(u):
        @pl.when(core == u % 2)
        def _():
            send(u, (0, 1))

    def feed_whole():
        near = 2 * level_of(far - 1)
        for c in range(2):
            for a in range(2):
                for n in range(width // tile):
                    cs = pl.ds(n * tile, tile)
                    whole[c, a, :, cs] = jnp.dot(
                        hot[blk(near + c)], xin[a, :, cs], preferred_element_type=F32).astype(BF16)
            full_copy(c, e, near + c).start()

    def compute(w):
        s = source(w)
        @pl.when(w == 1)
        def _():
            m_copy(mate).wait_recv()
            w_mate(mate).wait_recv()
        if far:
            @pl.when(w == 2)
            def _():
                some = pw_in.at[pl.ds(0, ep - 2)]
                remote(some, some, w_send, w_recv.at[0], mate, j).wait_recv()
            if crossed:
                @pl.when(w == 2)
                def _():
                    for bit in (1, 2):
                        cross_copy(bit, s, True).wait_recv()
                    diag_copy(0, s, s).wait_recv()
            @pl.when(w == units - 2)
            def _():
                full_copy(0, s, s).wait_recv()
            u = jnp.where(w == units - 1, spread_end - 1, w - 2)
            @pl.when(jnp.logical_and(w != units - 2, w >= 2 + first_spread))
            def _():
                for a in range(2):
                    gather_wait(a, u, s, nb - 1)
        x = rows[0, blk(s), :]
        pre_gate = lax.dot_general(x, weights[0], NT, preferred_element_type=F32)
        pre_up = lax.dot_general(x, weights[1], NT, preferred_element_type=F32)
        back = lax.dot_general(rows[1, blk(s), :], weights[2], NT, preferred_element_type=F32)
        p = jnp.broadcast_to(pw_in[s], (8, t_rows)).T[:cap, 0:1]
        sigma = jax.nn.sigmoid(pre_gate)
        silu = pre_gate * sigma
        hidden = silu * pre_up
        scaled = p * back
        gg = (scaled * pre_up * sigma * (1.0 + pre_gate * (1.0 - sigma))).astype(BF16)
        gu = (scaled * silu).astype(BF16)
        for n in range(width // tile):
            cs = pl.ds(n * tile, tile)
            part[s, :, cs] = (
                jnp.dot(gg, weights[0, :, cs], preferred_element_type=F32)
                + jnp.dot(gu, weights[1, :, cs], preferred_element_type=F32)).astype(BF16)
        for copy, _, _ in scatter_step(w, s, 0):
            copy.start()
        grads[0, blk(s)] = gg
        grads[1, blk(s)] = gu
        grads[2, blk(s)] = (p * hidden).astype(BF16)
        prod = jnp.sum(hidden * back, axis=1, keepdims=True)
        r_send[s, :, :cap] = jnp.broadcast_to(prod, (cap, t_rows)).T[0:1]
        @pl.when(w >= 1)
        def _():
            r_copy(s, e).start()
        @pl.when(w == 0)
        def _():
            r_in[e] = r_send[e]

    def merge(w, n):
        s = source(w)
        scatter_wait(w, n)
        for _, mine, got in scatter_step(w, s, n):
            mine[...] = (mine[...].astype(F32) + got[...].astype(F32)).astype(BF16)
        if n + 1 < nb:
            for copy, _, _ in scatter_step(w, s, n + 1):
                copy.start()
        else:
            @pl.when(w >= 1)
            def _():
                pz_copy(s, e).start()
            @pl.when(w == 0)
            def _():
                z_in[blk(e)] = part[e, :, col(j)]

    outs = (gate_out, up_out, down_out)

    def weight_grad(k):
        left = grads[k].T
        for n in range(width // tile):
            cs = pl.ds(n * tile, tile)
            outs[k][:, cs] = jnp.dot(left, rows[k // 2, :, cs], preferred_element_type=F32)

    def rt_copy(d, s):
        return remote(r_in, r_tp.at[s], rt_send, rt_recv, e, d)

    def rt_start(n, _):
        rt_copy(lax.rem(j + n, tp), j).start()
        return 0

    final = units + nb - 2

    bulk = units + nb - 3

    def done(t):
        count = jnp.where(t > bulk, units, jnp.clip(t - nb, 2, units))
        return jnp.where(t < 2, jnp.maximum(t, 0), count)

    def span_of(f, low, high):
        def one(w, _):
            f(w)
            return 0

        lax.fori_loop(low, high, one, 0)

    def merges(t, when):
        @pl.when(when)
        def _():
            for n in range(nb - 1, -1, -1):
                late = functools.partial(merge, n=n)
                if n == 0:
                    span_of(late, done(t - 1), done(t))
                else:
                    span_of(late, jnp.minimum(done(t - 2 - n), 2), jnp.minimum(done(t - 1 - n), 2))
                    span_of(late, jnp.maximum(done(t - 1 - n), 2), jnp.maximum(done(t - n), 2))
            @pl.when(t == final)
            def _():
                lines = r_in.at[pl.ds(0, ep - 1)]
                remote(lines, lines, rs_send, rs_recv, mate, j).wait()
                lax.fori_loop(1, tp, rt_start, 0)
                r_tp[j] = r_in[...]
                for k in range(0):
                    weight_grad(k)

    def tick(t, _):
        def stage_of(f, i, low, high):
            @pl.when(jnp.logical_and(i >= low, i < high))
            def _():
                f(i)

        if far:
            stage_of(feed, jnp.where(t > 2, t, 0), 2, far - 1)
            @pl.when(jnp.logical_and(t == max(1, far - 3), core == 1))
            def _():
                feed_whole()
        merges(t, t >= bulk - 1)
        span_of(compute, done(t), done(t + 1))
        if far:
            stage_of(feed, jnp.where(t == 1, 2, 0), 2, far - 1)
            stage_of(arrive, jnp.where(t <= 2, t - 1, -1), 0, far - 1)
        merges(t, t < bulk - 1)
        if far:
            for n in range(1, nb):
                stage_of(functools.partial(spread, n=n), t - 1 - n, first_spread, spread_end)
            stage_of(arrive, jnp.where(t > 2, t - 1, -1), 0, far - 1)
        return 0

    lax.fori_loop(0, units + 2 * nb - 2, tick, 0)
    for k in range(0, 3):
        weight_grad(k)
    hot_t[...] = hot[...].T
    lines = r_tp.at[pl.ds(0, tp - 1)]
    remote(lines, lines, rt_send, rt_recv, e, flip(1)).wait()
    for x in range(ep):
        total = r_tp[0, x]
        for i in range(1, tp):
            total = total + r_tp[i, x]
        r_mat[x:x + 1, :cap] = total[:, :cap]
    sums = r_mat[...].T
    found = [jnp.zeros((1, t_rows), F32) for _ in range(2)]
    for x in range(ep):
        value = jnp.sum(
            hot[x * cap:(x + 1) * cap].astype(F32) * sums[:cap, x:x + 1], axis=0, keepdims=True)
        found = [f + jnp.where(idr[k:k + 1] == x, value, 0.0) for k, f in enumerate(found)]
    for k in range(2):
        route_out[k:k + 1] = found[k]

    lines = pw_out.at[pl.ds(0, ep - 1)]
    remote(lines, lines, w_send, w_recv.at[0], mate, j).wait_send()
    m_copy(e).wait_send()
    if far:
        @pl.when(core == 0)
        def _():
            sent = stage.at[:, :far * cap]
            remote(sent, sent, z_send, z_recv.at[0, 0], mate, j).wait_send()
            if crossed:
                remote(diag, diag, d_send, d_recv, mate, j).wait_send()
        @pl.when(core == 1)
        def _():
            if far > 2:
                sent = stage.at[:, :(far - 2) * cap]
                remote(sent, sent, z_send, z_recv.at[0, 0], mate, j).wait_send()
            remote(whole, whole, f_send, f_recv, mate, j).wait_send()
        if crossed:
            sent = rows.at[:, :cap, :2 * span]
            remote(sent, sent, x_send, x_recv.at[0], e, flip(1)).wait_send()
        if spreads:
            sent = rows.at[:, :spreads * cap, :(tp - 1) * span]
            remote(sent, sent, t_send, t_recv.at[0, 0, 0], e, flip(1)).wait_send()
    sent = part.at[:, :, :(tp - 1) * span]
    remote(sent, sent, p_send, p_recv.at[0, 0], e, flip(1)).wait_send()
    sent = z_in.at[:(ep - 1) * cap]
    remote(sent, sent, pz_send, pz_recv, mate, j).wait()
    dx_out[...] = jnp.dot(hot_t[...], z_in[...], preferred_element_type=F32).astype(BF16)


def publish(*refs):
    srcs, dsts, sem = refs[:5], refs[5:10], refs[10]
    copies = [pltpu.make_async_copy(srcs[k], dsts[k], sem.at[k]) for k in (2, 3, 4, 0, 1)]
    for copy in copies:
        copy.start()
    for copy in copies:
        copy.wait()


def per_device(tokens, cotangent, expert_ids, route_weight, gate_weight, up_weight, down_weight):
    ep, tp = lax.axis_size("ep"), lax.axis_size("tp")
    t_rows, width = tokens.shape
    top = expert_ids.shape[1]
    _, f_rows, _ = gate_weight.shape
    cap = min(t_rows, 2 * top * t_rows // ep)
    span = width // tp
    nb = tp.bit_length() - 1
    any_, vmem = pl.BlockSpec(memory_space=pl.ANY), pl.BlockSpec(memory_space=pltpu.VMEM)
    dma = pltpu.SemaphoreType.DMA
    big = pltpu.VMEM((f_rows, width), F32)
    scratch = [
        pltpu.VMEM(expert_ids.shape[::-1], jnp.int32),
        pltpu.VMEM(route_weight.shape[::-1], route_weight.dtype),
        pltpu.VMEM((2, t_rows, width), BF16),
        pltpu.VMEM((ep * cap, t_rows), BF16),
        pltpu.VMEM((t_rows, ep * cap), BF16),
        pltpu.VMEM((2, ep * cap, span), BF16),
        pltpu.VMEM((2, cap, width), BF16),
        pltpu.VMEM((2, 2, cap, width), BF16),
        pltpu.VMEM((2, 2, cap, span), BF16),
        pltpu.VMEM((2, ep * cap, width), BF16),
        pltpu.VMEM((3, f_rows, width), BF16),
        pltpu.VMEM((ep, 1, t_rows), F32),
        pltpu.VMEM((ep, 1, t_rows), F32),
        pltpu.VMEM((3, ep * cap, f_rows), BF16),
        pltpu.VMEM((ep, cap, width), BF16),
        pltpu.VMEM((ep, cap // 2, (tp - 1) * span), BF16),
        pltpu.VMEM((ep, tp - 1, cap // 2, span), BF16),
        pltpu.VMEM((ep * cap, span), BF16),
        pltpu.VMEM((ep, 1, t_rows), F32),
        pltpu.VMEM((ep, 1, t_rows), F32),
        pltpu.VMEM((tp, ep, 1, t_rows), F32),
        pltpu.VMEM((ep, t_rows), F32),
        dma((7,)), dma(()), dma((2, max(ep - 3, 1))), dma(()), dma(()), dma(()), dma(()),
        dma(()), dma((2,)), dma(()), dma(()), dma(()), dma((2,)),
        dma(()), dma((2, max(ep - 3, 1), nb)), dma(()), dma((ep, nb)), dma(()), dma(()),
        dma(()), dma(()), dma(()), dma(()),
    ]
    pieces = pl.pallas_call(
        functools.partial(kernel, ep, tp, cap),
        out_shape=(
            pltpu.VMEM((t_rows, span), BF16),
            pltpu.VMEM(expert_ids.shape[::-1], F32), big, big, big),
        in_specs=[any_] * 7,
        out_specs=(vmem,) * 5,
        scratch_shapes=scratch,
        compiler_params=pltpu.CompilerParams(
            collective_id=0, has_side_effects=True,
            vmem_limit_bytes=VMEM_BYTES - 12 * f_rows * width - 2 * t_rows * span),
    )(tokens, cotangent, expert_ids.T, route_weight.T, gate_weight[0], up_weight[0], down_weight[0])
    dx, route, *wide = pl.pallas_call(
        publish,
        out_shape=tuple(jax.ShapeDtypeStruct(v.shape, v.dtype) for v in pieces),
        in_specs=[vmem] * 5,
        out_specs=(any_,) * 5,
        scratch_shapes=[dma((5,))],
        compiler_params=pltpu.CompilerParams(vmem_limit_bytes=1_000_000),
    )(*(pltpu.with_memory_space_constraint(v, pltpu.VMEM) for v in pieces))
    return dx, route.T, *(g[None] for g in wide)


def solution(mesh):
    in_specs = (
        P("ep", None), P("ep", None), P("ep", None), P("ep", None),
        P("ep", "tp", None), P("ep", "tp", None), P("ep", "tp", None),
    )
    out_specs = (
        P("ep", "tp"), P("ep", None), P("ep", "tp", None), P("ep", "tp", None), P("ep", "tp", None),
    )
    return jax.shard_map(
        per_device, mesh=mesh, in_specs=in_specs, out_specs=out_specs, check_vma=False
    )
```

time: 65.1 us -> 62.4 us (0.959); the launches traced: 64.3 us -> 62.3 us
  Pallas kernels: 63.7 us -> 61.6 us
    pallas_call x1, Pallas kernels: 60.9 us -> 58.9 us  [per_device(): pl.pallas_call(functools.partial(kernel, ep, tp, cap), out_shape=(pltpu.V...]
where the time goes in v3:
time: 62.4 us; the launch traced here: 62.3 us
  Pallas kernels  61.6 us (99%)
  between operations  0.64 us (1%)
    pallas_call x1, Pallas kernels, per_device(): pl.pallas_call(functools.partial(kernel, ep, tp, cap), out_shape=(pltpu.V...  58.9 us
    pallas_call x1, Pallas kernels, per_device(): pl.pallas_call(publish, out_shape=tuple((jax.ShapeDtypeStruct(v.shape, v....  2.75 us

profile of v3, /device:TPU:0, one launch (start us, length us, event | category | flops | bytes accessed | tf_op | source)
XLA Modules:
  0.0 62.3 jit_solution(13561535264408431374)
XLA Ops:
  0.6 58.9 %shard_map.110 = (bf16[128,512]{1,0:T(8,128)(2,1)S(1)}, f32[2,128]{1,0:T(2,128)S(1)}, f32[256,2048]{1,0:T(8,128)S(1)}, f32[256,2048]{1,0:T(8,128)S(1)}, f32[256,2048]{1,0:T(8,128)S(1)}) custom-call(bf16[128,2048]{1,0:T(8,128)(2,1)} %tokens.1, bf16[128,2048]{1,0:T(8,128)(2,1)} %cotangent.1, s32[2,128]{1,0:T(2,128)} %bitcast.12, bf16[2,128]{1,0:T(2,128)(2,1)} %bitcast.13, ...), custom_call_target="tpu_custom_call" | custom-call | tf_op jit(solution)/shard_map/pallas_call | solution.py:530
  59.5 2.7 %shard_map.111 = (bf16[128,512]{1,0:T(8,128)(2,1)}, f32[2,128]{1,0:T(2,128)}, f32[256,2048]{1,0:T(8,128)}, f32[256,2048]{1,0:T(8,128)}, f32[256,2048]{1,0:T(8,128)}) custom-call(bf16[128,512]{1,0:T(8,128)(2,1)S(1)} %get-tuple-element.15.refs_0_, f32[2,128]{1,0:T(2,128)S(1)} %get-tuple-element.16.refs_1_, f32[256,2048]{1,0:T(8,128)S(1)} %get-tuple-element.17.refs_2_, ...), custom_call_target="tpu_custom_call" | custom-call | tf_op jit(solution)/shard_map/pallas_call | solution.py:542

commit v4 on v3

--- a/solution.py
+++ b/solution.py
@@ -28,7 +28,7 @@
 def kernel(
     ep, tp, cap, tokens, cotangent, ids_in, probs_in, gate_w, up_w, down_w,
     dx_out, route_out, gate_out, up_out, down_out,
-    ids, probs, xin, hot, hot_t, stage, mate_rows, whole, diag, rows, weights, pw_out, pw_in, grads, part, ta_in, tb_in, z_in,
+    ids, probs, xin, hot, hot_t, stage, mate_rows, whole, diag, rows, weights, flipped, pw_out, pw_in, grads, part, ta_in, tb_in, z_in,
     r_send, r_in, r_tp, r_mat,
     load_sem, z_send, z_recv, m_send, m_recv, f_send, f_recv, x_send, x_recv, d_send, d_recv,
     w_send, w_recv, t_send, t_recv, p_send, p_recv, pz_send, pz_recv, rs_send, rs_recv,
@@ -45,10 +45,8 @@
     lb = levels.bit_length() - 1
     far = 2 * (levels - 1)
     units = far + 2
-    crossed = False
-    first_spread = 1 if crossed else 0
-    spread_end = far - 1
-    spreads = spread_end - first_spread
+    crossed = tp == 4 and far > 2
+    spread_end = far - 2 if crossed else far - 1
     tile = min(width, 512)
 
     def xor(a, b):
@@ -62,8 +60,13 @@
         d = u // 2 + 1 + u % 2
         return xor(lvl, jnp.where(d >= levels, 1, d))
 
+    whole_at = units - 3 if far > 2 else units - 1
+
+    def unit_of(w):
+        return jnp.where(w == whole_at, units - 1, jnp.where(w > whole_at, w - 1, w))
+
     def source(w):
-        v = jnp.where(w == units - 2, units - 1, jnp.where(w == units - 1, units - 2, w)) if far else w
+        v = unit_of(w)
         u = jnp.maximum(v - 2, 0)
         return jnp.where(v == 0, e, jnp.where(v == 1, mate, 2 * level_of(u) + u % 2))
 
@@ -235,18 +238,12 @@
     if far:
         send(core, (0, 1))
     m_copy(e).start()
-    if crossed:
-        @pl.when(core == 0)
-        def _():
-            for a in range(2):
-                for c in range(2):
-                    diag[c, a] = jnp.dot(
-                        hot[blk(2 * level_of(0) + c)], xin[a, :, col(tp - 1 - j)],
-                        preferred_element_type=F32).astype(BF16)
-            for c in range(2):
-                diag_copy(c, e, 2 * level_of(0) + c).start()
-    for n in range(2, 5):
-        loads[n].wait()
+
+    for k in range(3):
+        loads[k + 2].wait()
+        for n in range(width // tile):
+            cs = pl.ds(n * tile, tile)
+            flipped[k, cs] = weights[k, :, cs].T
 
     def source_of(u):
         return 2 * level_of(u) + u % 2
@@ -255,12 +252,12 @@
         s = source_of(u)
         for a in range(2):
             z_wait(a, u, s).wait_recv()
-            @pl.when(u >= first_spread)
+            @pl.when(u < spread_end)
             def _():
                 for copy in gather_step(a, u, s, 0):
                     copy.start()
         if crossed:
-            @pl.when(u == 0)
+            @pl.when(u == spread_end)
             def _():
                 for bit in (1, 2):
                     cross_copy(bit, s, False).start()
@@ -276,6 +273,15 @@
         @pl.when(core == u % 2)
         def _():
             send(u, (0, 1))
+
+    def feed_cross():
+        there = 2 * level_of(spread_end)
+        for c in range(2):
+            for a in range(2):
+                diag[c, a] = jnp.dot(
+                    hot[blk(there + c)], xin[a, :, col(tp - 1 - j)],
+                    preferred_element_type=F32).astype(BF16)
+            diag_copy(c, e, there + c).start()
 
     def feed_whole():
         near = 2 * level_of(far - 1)
@@ -299,23 +305,23 @@
                 some = pw_in.at[pl.ds(0, ep - 2)]
                 remote(some, some, w_send, w_recv.at[0], mate, j).wait_recv()
             if crossed:
-                @pl.when(w == 2)
+                @pl.when(w == units - 1)
                 def _():
                     for bit in (1, 2):
                         cross_copy(bit, s, True).wait_recv()
                     diag_copy(0, s, s).wait_recv()
-            @pl.when(w == units - 2)
+            @pl.when(w == whole_at)
             def _():
                 full_copy(0, s, s).wait_recv()
-            u = jnp.where(w == units - 1, spread_end - 1, w - 2)
-            @pl.when(jnp.logical_and(w != units - 2, w >= 2 + first_spread))
+            u = unit_of(w) - 2
+            @pl.when(jnp.logical_and(w != whole_at, jnp.logical_and(w >= 2, u < spread_end)))
             def _():
                 for a in range(2):
                     gather_wait(a, u, s, nb - 1)
         x = rows[0, blk(s), :]
-        pre_gate = lax.dot_general(x, weights[0], NT, preferred_element_type=F32)
-        pre_up = lax.dot_general(x, weights[1], NT, preferred_element_type=F32)
-        back = lax.dot_general(rows[1, blk(s), :], weights[2], NT, preferred_element_type=F32)
+        pre_gate = jnp.dot(x, flipped[0], preferred_element_type=F32)
+        pre_up = jnp.dot(x, flipped[1], preferred_element_type=F32)
+        back = jnp.dot(rows[1, blk(s), :], flipped[2], preferred_element_type=F32)
         p = jnp.broadcast_to(pw_in[s], (8, t_rows)).T[:cap, 0:1]
         sigma = jax.nn.sigmoid(pre_gate)
         silu = pre_gate * sigma
@@ -373,7 +379,6 @@
         rt_copy(lax.rem(j + n, tp), j).start()
         return 0
 
-    final = units + nb - 2
 
     bulk = units + nb - 3
 
@@ -398,14 +403,12 @@
                 else:
                     span_of(late, jnp.minimum(done(t - 2 - n), 2), jnp.minimum(done(t - 1 - n), 2))
                     span_of(late, jnp.maximum(done(t - 1 - n), 2), jnp.maximum(done(t - n), 2))
-            @pl.when(t == final)
-            def _():
-                lines = r_in.at[pl.ds(0, ep - 1)]
-                remote(lines, lines, rs_send, rs_recv, mate, j).wait()
-                lax.fori_loop(1, tp, rt_start, 0)
-                r_tp[j] = r_in[...]
-                for k in range(0):
-                    weight_grad(k)
+
+    def exchange():
+        lines = r_in.at[pl.ds(0, ep - 1)]
+        remote(lines, lines, rs_send, rs_recv, mate, j).wait()
+        lax.fori_loop(1, tp, rt_start, 0)
+        r_tp[j] = r_in[...]
 
     def tick(t, _):
         def stage_of(f, i, low, high):
@@ -415,22 +418,43 @@
 
         if far:
             stage_of(feed, jnp.where(t > 2, t, 0), 2, far - 1)
+            if crossed:
+                @pl.when(jnp.logical_and(t == spread_end + 1, core == 0))
+                def _():
+                    feed_cross()
             @pl.when(jnp.logical_and(t == max(1, far - 3), core == 1))
             def _():
                 feed_whole()
+        if far > 2:
+            @pl.when(t == bulk)
+            def _():
+                span_of(compute, whole_at, whole_at + 2)
         merges(t, t >= bulk - 1)
-        span_of(compute, done(t), done(t + 1))
+        span_of(compute, done(t) + jnp.where(t == bulk, 2, 0) if far > 2 else done(t), done(t + 1))
         if far:
             stage_of(feed, jnp.where(t == 1, 2, 0), 2, far - 1)
             stage_of(arrive, jnp.where(t <= 2, t - 1, -1), 0, far - 1)
         merges(t, t < bulk - 1)
         if far:
             for n in range(1, nb):
-                stage_of(functools.partial(spread, n=n), t - 1 - n, first_spread, spread_end)
+                stage_of(functools.partial(spread, n=n), t - 1 - n, 0, spread_end)
             stage_of(arrive, jnp.where(t > 2, t - 1, -1), 0, far - 1)
         return 0
 
-    lax.fori_loop(0, units + 2 * nb - 2, tick, 0)
+    if far > 2 and nb == 2:
+        lax.fori_loop(0, bulk + 1, tick, 0)
+        halves, wholes = functools.partial(merge, n=0), functools.partial(merge, n=1)
+        last = units - 1
+        span_of(halves, last - 2, last)
+        span_of(wholes, last - 3, last - 2)
+        span_of(halves, last, units)
+        span_of(wholes, last - 1, last)
+        exchange()
+        span_of(wholes, last - 2, last - 1)
+        span_of(wholes, last, units)
+    else:
+        lax.fori_loop(0, units + 2 * nb - 2, tick, 0)
+        exchange()
     for k in range(0, 3):
         weight_grad(k)
     hot_t[...] = hot[...].T
@@ -469,8 +493,8 @@
         if crossed:
             sent = rows.at[:, :cap, :2 * span]
             remote(sent, sent, x_send, x_recv.at[0], e, flip(1)).wait_send()
-        if spreads:
-            sent = rows.at[:, :spreads * cap, :(tp - 1) * span]
+        if spread_end:
+            sent = rows.at[:, :spread_end * cap, :(tp - 1) * span]
             remote(sent, sent, t_send, t_recv.at[0, 0, 0], e, flip(1)).wait_send()
     sent = part.at[:, :, :(tp - 1) * span]
     remote(sent, sent, p_send, p_recv.at[0, 0], e, flip(1)).wait_send()
@@ -511,6 +535,7 @@
         pltpu.VMEM((2, 2, cap, span), BF16),
         pltpu.VMEM((2, ep * cap, width), BF16),
         pltpu.VMEM((3, f_rows, width), BF16),
+        pltpu.VMEM((3, width, f_rows), BF16),
         pltpu.VMEM((ep, 1, t_rows), F32),
         pltpu.VMEM((ep, 1, t_rows), F32),
         pltpu.VMEM((3, ep * cap, f_rows), BF16),

time: 62.4 us -> 60 us (0.962)
  Pallas kernels: 61.6 us -> 59.2 us
    pallas_call x1, Pallas kernels: 58.9 us -> 56.4 us  [per_device(): pl.pallas_call(functools.partial(kernel, ep, tp, cap), out_shape=(pltpu.V...]
where the time goes in v4:
time: 60 us; the launch traced here: 59.8 us
  Pallas kernels  59.2 us (99%)
  between operations  0.64 us (1%)
    pallas_call x1, Pallas kernels, per_device(): pl.pallas_call(functools.partial(kernel, ep, tp, cap), out_shape=(pltpu.V...  56.4 us
    pallas_call x1, Pallas kernels, per_device(): pl.pallas_call(publish, out_shape=tuple((jax.ShapeDtypeStruct(v.shape, v....  2.75 us

profile of v4, /device:TPU:0, one launch (start us, length us, event | category | flops | bytes accessed | tf_op | source)
XLA Modules:
  0.0 59.8 jit_solution(4668467366938089801)
XLA Ops:
  0.6 56.4 %shard_map.110 = (bf16[128,512]{1,0:T(8,128)(2,1)S(1)}, f32[2,128]{1,0:T(2,128)S(1)}, f32[256,2048]{1,0:T(8,128)S(1)}, f32[256,2048]{1,0:T(8,128)S(1)}, f32[256,2048]{1,0:T(8,128)S(1)}) custom-call(bf16[128,2048]{1,0:T(8,128)(2,1)} %tokens.1, bf16[128,2048]{1,0:T(8,128)(2,1)} %cotangent.1, s32[2,128]{1,0:T(2,128)} %bitcast.12, bf16[2,128]{1,0:T(2,128)(2,1)} %bitcast.13, ...), custom_call_target="tpu_custom_call" | custom-call | tf_op jit(solution)/shard_map/pallas_call | solution.py:555
  57.1 2.7 %shard_map.111 = (bf16[128,512]{1,0:T(8,128)(2,1)}, f32[2,128]{1,0:T(2,128)}, f32[256,2048]{1,0:T(8,128)}, f32[256,2048]{1,0:T(8,128)}, f32[256,2048]{1,0:T(8,128)}) custom-call(bf16[128,512]{1,0:T(8,128)(2,1)S(1)} %get-tuple-element.15.refs_0_, f32[2,128]{1,0:T(2,128)S(1)} %get-tuple-element.16.refs_1_, f32[256,2048]{1,0:T(8,128)S(1)} %get-tuple-element.17.refs_2_, ...), custom_call_target="tpu_custom_call" | custom-call | tf_op jit(solution)/shard_map/pallas_call | solution.py:567

commit v5 on v4

--- a/solution.py
+++ b/solution.py
@@ -211,32 +211,33 @@
     for a in range(2):
         loads[a].wait()
         select(a)
+
+    p = probs[...].astype(F32)
+    chosen = (jnp.where(first, p[0:1], 0.0) + jnp.where(second, p[1:2], 0.0)).astype(BF16)
+    slot_p = lax.dot_general(chosen, hot[...], NT, preferred_element_type=F32)
+    for x in range(ep):
+        pw_out[x, :, :cap] = slot_p[x:x + 1, x * cap:(x + 1) * cap]
+    pw_in[e] = pw_out[e]
+
+    def w_start(n, _):
+        d = lax.rem(e + n, ep)
+        @pl.when(d != mate)
+        def _():
+            w_copy(d, e).start()
+        return 0
+
+    pl.semaphore_wait(barrier, ep + tp - 2)
+    lax.fori_loop(1, ep, w_start, 0)
+    w_mate(e).start()
+    if far:
+        send(core, (0, 1))
+    for a in range(2):
         for n in range(width // tile):
             cs = pl.ds(n * tile, tile)
             mate_rows[a, :, cs] = jnp.dot(
                 hot[blk(mate)], xin[a, :, cs], preferred_element_type=F32).astype(BF16)
             rows[a, blk(e), cs] = jnp.dot(
                 hot[blk(e)], xin[a, :, cs], preferred_element_type=F32).astype(BF16)
-
-    p = probs[...].astype(F32)
-    chosen = (jnp.where(first, p[0:1], 0.0) + jnp.where(second, p[1:2], 0.0)).astype(BF16)
-    slot_p = lax.dot_general(chosen, hot[...], NT, preferred_element_type=F32)
-    for x in range(ep):
-        pw_out[x, :, :cap] = slot_p[x:x + 1, x * cap:(x + 1) * cap]
-    pw_in[e] = pw_out[e]
-
-    def w_start(n, _):
-        d = lax.rem(e + n, ep)
-        @pl.when(d != mate)
-        def _():
-            w_copy(d, e).start()
-        return 0
-
-    pl.semaphore_wait(barrier, ep + tp - 2)
-    lax.fori_loop(1, ep, w_start, 0)
-    w_mate(e).start()
-    if far:
-        send(core, (0, 1))
     m_copy(e).start()
 
     for k in range(3):
@@ -449,9 +450,9 @@
         span_of(wholes, last - 3, last - 2)
         span_of(halves, last, units)
         span_of(wholes, last - 1, last)
-        exchange()
         span_of(wholes, last - 2, last - 1)
         span_of(wholes, last, units)
+        exchange()
     else:
         lax.fori_loop(0, units + 2 * nb - 2, tick, 0)
         exchange()

time: 60 us -> 59.6 us (level)
  no operation moved by 1% of the time
where the time goes in v5:
time: 59.6 us; the launch traced here: 59.4 us
  Pallas kernels  58.8 us (99%)
  between operations  0.64 us (1%)
    pallas_call x1, Pallas kernels, per_device(): pl.pallas_call(functools.partial(kernel, ep, tp, cap), out_shape=(pltpu.V...  56 us
    pallas_call x1, Pallas kernels, per_device(): pl.pallas_call(publish, out_shape=tuple((jax.ShapeDtypeStruct(v.shape, v....  2.75 us

profile of v5, /device:TPU:0, one launch (start us, length us, event | category | flops | bytes accessed | tf_op | source)
XLA Modules:
  0.0 59.4 jit_solution(16869376025946384418)
XLA Ops:
  0.6 56.0 %shard_map.110 = (bf16[128,512]{1,0:T(8,128)(2,1)S(1)}, f32[2,128]{1,0:T(2,128)S(1)}, f32[256,2048]{1,0:T(8,128)S(1)}, f32[256,2048]{1,0:T(8,128)S(1)}, f32[256,2048]{1,0:T(8,128)S(1)}) custom-call(bf16[128,2048]{1,0:T(8,128)(2,1)} %tokens.1, bf16[128,2048]{1,0:T(8,128)(2,1)} %cotangent.1, s32[2,128]{1,0:T(2,128)} %bitcast.12, bf16[2,128]{1,0:T(2,128)(2,1)} %bitcast.13, ...), custom_call_target="tpu_custom_call" | custom-call | tf_op jit(solution)/shard_map/pallas_call | solution.py:556
  56.7 2.7 %shard_map.111 = (bf16[128,512]{1,0:T(8,128)(2,1)}, f32[2,128]{1,0:T(2,128)}, f32[256,2048]{1,0:T(8,128)}, f32[256,2048]{1,0:T(8,128)}, f32[256,2048]{1,0:T(8,128)}) custom-call(bf16[128,512]{1,0:T(8,128)(2,1)S(1)} %get-tuple-element.15.refs_0_, f32[2,128]{1,0:T(2,128)S(1)} %get-tuple-element.16.refs_1_, f32[256,2048]{1,0:T(8,128)S(1)} %get-tuple-element.17.refs_2_, ...), custom_call_target="tpu_custom_call" | custom-call | tf_op jit(solution)/shard_map/pallas_call | solution.py:568

commit v6 on v5

--- a/solution.py
+++ b/solution.py
@@ -236,9 +236,12 @@
             cs = pl.ds(n * tile, tile)
             mate_rows[a, :, cs] = jnp.dot(
                 hot[blk(mate)], xin[a, :, cs], preferred_element_type=F32).astype(BF16)
+    m_copy(e).start()
+    for a in range(2):
+        for n in range(width // tile):
+            cs = pl.ds(n * tile, tile)
             rows[a, blk(e), cs] = jnp.dot(
                 hot[blk(e)], xin[a, :, cs], preferred_element_type=F32).astype(BF16)
-    m_copy(e).start()
 
     for k in range(3):
         loads[k + 2].wait()

time: 59.6 us -> 59.5 us (level)
  no operation moved by 1% of the time
where the time goes in v6:
time: 59.5 us; the launch traced here: 59.4 us
  Pallas kernels  58.7 us (99%)
  between operations  0.64 us (1%)
    pallas_call x1, Pallas kernels, per_device(): pl.pallas_call(functools.partial(kernel, ep, tp, cap), out_shape=(pltpu.V...  56 us
    pallas_call x1, Pallas kernels, per_device(): pl.pallas_call(publish, out_shape=tuple((jax.ShapeDtypeStruct(v.shape, v....  2.75 us

profile of v6, /device:TPU:0, one launch (start us, length us, event | category | flops | bytes accessed | tf_op | source)
XLA Modules:
  0.0 59.4 jit_solution(6876504713087775419)
XLA Ops:
  0.6 56.0 %shard_map.110 = (bf16[128,512]{1,0:T(8,128)(2,1)S(1)}, f32[2,128]{1,0:T(2,128)S(1)}, f32[256,2048]{1,0:T(8,128)S(1)}, f32[256,2048]{1,0:T(8,128)S(1)}, f32[256,2048]{1,0:T(8,128)S(1)}) custom-call(bf16[128,2048]{1,0:T(8,128)(2,1)} %tokens.1, bf16[128,2048]{1,0:T(8,128)(2,1)} %cotangent.1, s32[2,128]{1,0:T(2,128)} %bitcast.12, bf16[2,128]{1,0:T(2,128)(2,1)} %bitcast.13, ...), custom_call_target="tpu_custom_call" | custom-call | tf_op jit(solution)/shard_map/pallas_call | solution.py:559
  56.6 2.7 %shard_map.111 = (bf16[128,512]{1,0:T(8,128)(2,1)}, f32[2,128]{1,0:T(2,128)}, f32[256,2048]{1,0:T(8,128)}, f32[256,2048]{1,0:T(8,128)}, f32[256,2048]{1,0:T(8,128)}) custom-call(bf16[128,512]{1,0:T(8,128)(2,1)S(1)} %get-tuple-element.15.refs_0_, f32[2,128]{1,0:T(2,128)S(1)} %get-tuple-element.16.refs_1_, f32[256,2048]{1,0:T(8,128)S(1)} %get-tuple-element.17.refs_2_, ...), custom_call_target="tpu_custom_call" | custom-call | tf_op jit(solution)/shard_map/pallas_call | solution.py:571
